TPU v7x, 32 devices: a whole 2x2x4 slice. The times are simulated.
32 devices in a mesh: sp: 4 (over z), fs: 4 (over y, x), tp: 2 (over core).
Axes of the slice: x: 2, y: 2, z: 4, core: 2. Of those that a mesh axis runs over, the one named last changes fastest.
Arguments:
- tokens: bfloat16 [4, 1024, 2048], P('fs', 'sp', 'tp'), may hold values from -6 to 6
- norm_gain: float32 [2048], replicated, may hold values from 0.1 to 1.9
- query_weight: bfloat16 [2048, 1024], P('fs', 'tp'), may hold values from -1 to 1
- key_weight: bfloat16 [2048, 1024], P('fs', 'tp'), may hold values from -4 to 4
- value_weight: bfloat16 [2048, 1024], P('fs', 'tp'), may hold values from -0.125 to 0.125
- state_query: bfloat16 [2048, 1024], P('fs', 'tp'), may hold values from -0.125 to 0.125
- state_key: bfloat16 [2048, 1024], P('fs', 'tp'), may hold values from -0.125 to 0.125
- state_value: bfloat16 [2048, 1024], P('fs', 'tp'), may hold values from -0.125 to 0.125
- map_lambda: float32 [8], P('tp'), may hold values from 0.3 to 0.8
- diff_gain: float32 [1024], P('tp'), may hold values from 0.1 to 1.9
- decay_rate: float32 [8], P('tp'), may hold values from 0 to 0.04
- state_gain: float32 [1024], P('tp'), may hold values from 0.1 to 1.9
- out_weight: bfloat16 [2048, 2048], replicated, may hold values from -0.125 to 0.125
Outputs:
- mixed: bfloat16 [4, 1024, 2048], P('fs', ('sp', 'tp'))
All inputs are finite; a program needn't handle non-finite values.
Results may differ from a plain program's by a relative error of at most 0.015.
Values may be sent and summed in bfloat16 or wider, within the bound.
A program may use at most 128 MiB of HBM per device.

v0:
```python
import functools

import jax
import jax.numpy as jnp
from jax import lax
from jax.experimental import pallas as pl
from jax.experimental.pallas import tpu as pltpu
from jax.sharding import PartitionSpec as P

DK = 64
DV = 128
DR = 128


epsilon = 1e-05
branch_scale = 0.8
masked_score = -1e30


def from_behind(x, axis, by):
    size = lax.axis_size(axis)
    pairs = [(i, i + by) for i in range(size) if 0 <= i + by < size]
    return lax.ppermute(x, axis, pairs)


def entering(x, axis, join, neutral):
    place = lax.axis_index(axis)
    gathered = jax.tree.map(
        lambda a, kind: lax.all_gather(a.astype(kind), axis), x, (jnp.bfloat16, jnp.bfloat16)
    )
    state = jax.tree.map(lambda a, e: jnp.zeros_like(a) + jnp.asarray(e, a.dtype), x, neutral)

    def one(turn, state):
        return join(
            state,
            jax.tree.map(
                lambda a, own: lax.dynamic_index_in_dim(a, turn, 0, False).astype(own.dtype),
                gathered,
                x,
            ),
        )

    return lax.fori_loop(0, place, one, state)


def attend(att_query, att_keys, att_values, map_lambda, diff_gain):
    tok_rows = att_query.shape[0]
    head_count = map_lambda.shape[0]
    key_width = att_keys.shape[1]
    query_heads = att_query.reshape(tok_rows, head_count, 2, DK)
    sp_index = lax.axis_index("sp")
    query_place = sp_index * tok_rows + jnp.arange(tok_rows)
    score_scale = DK ** (-0.5)

    def absorb_block(running, inputs):
        key_block, key_place = inputs
        key_heads = key_block[:, :key_width].reshape(tok_rows, head_count, 2, DK)
        value_heads = key_block[:, key_width:].reshape(tok_rows, head_count, DV)
        scores = (
            jnp.einsum(
                "qhmd,khmd->mhqk", query_heads, key_heads, preferred_element_type=jnp.float32
            )
            * score_scale
        )
        causal = key_place[None, :] <= query_place[:, None]
        row_peak, totals, summed = running
        new_peak = jnp.maximum(row_peak, jnp.max(jnp.where(causal, scores, masked_score), axis=-1))
        weights = jnp.where(causal, jnp.exp(scores - new_peak[..., None]), 0.0)
        factor = jnp.exp(row_peak - new_peak)
        totals = totals * factor + jnp.sum(weights, axis=-1)
        summed = summed * factor[..., None] + jnp.einsum(
            "mhqk,khv->mhqv",
            weights.astype(jnp.bfloat16),
            value_heads,
            preferred_element_type=jnp.float32,
        )
        return ((new_peak, totals, summed), None)

    def absorb(running, pieces, first_row):
        piece_rows = pieces.shape[0]
        stacked = pieces.reshape(piece_rows // tok_rows, tok_rows, pieces.shape[1])
        places = (first_row + jnp.arange(piece_rows)).reshape(piece_rows // tok_rows, tok_rows)
        return lax.scan(absorb_block, running, (stacked, places))[0]

    starting = (
        jnp.full((2, head_count, tok_rows), masked_score, jnp.float32),
        jnp.zeros((2, head_count, tok_rows), jnp.float32),
        jnp.zeros((2, head_count, tok_rows, DV), jnp.float32),
    )
    joined_kv = jnp.concatenate([att_keys, att_values], axis=1)
    first_state = absorb(starting, joined_kv, sp_index * tok_rows)

    def relay_step(step_index, relay_state):
        running, moving = relay_state
        moving = from_behind(moving, "sp", 1)
        first_row = (sp_index - step_index) * tok_rows
        running = lax.cond(
            first_row >= 0,
            lambda holding: absorb(holding, moving, first_row),
            lambda holding: holding,
            running,
        )
        return (running, moving)

    running, _ = lax.fori_loop(1, lax.axis_size("sp"), relay_step, (first_state, joined_kv))
    row_peak, totals, summed = running
    averaged = summed / totals[..., None]
    differ = averaged[0] - map_lambda[:, None, None] * averaged[1]
    normed = differ * lax.rsqrt(jnp.mean(differ * differ, axis=-1, keepdims=True) + epsilon)
    normed = normed * diff_gain.reshape(head_count, 1, DV) * branch_scale
    return normed.transpose(1, 0, 2).reshape(tok_rows, head_count * DV).astype(jnp.bfloat16)


def retain(ret_query, ret_keys, ret_values, decay_rate, state_gain):
    tok_rows = ret_query.shape[0]
    head_count = decay_rate.shape[0]
    query_heads = ret_query.reshape(tok_rows, head_count, DR)
    key_heads = ret_keys.reshape(tok_rows, head_count, DR)
    value_heads = ret_values.reshape(tok_rows, head_count, DR)
    position = jnp.arange(tok_rows).astype(jnp.float32)
    distance = position[:, None] - position[None, :]
    decay_col = decay_rate[:, None, None]
    within = jnp.where(distance >= 0, jnp.exp(-decay_col * jnp.maximum(distance, 0.0)), 0.0)
    local_scores = (
        jnp.einsum("qhd,khd->hqk", query_heads, key_heads, preferred_element_type=jnp.float32)
        * within
    )
    intra_out = jnp.einsum(
        "hqk,khv->hqv",
        local_scores.astype(jnp.bfloat16),
        value_heads,
        preferred_element_type=jnp.float32,
    )
    key_decayed = key_heads.astype(jnp.float32) * jnp.exp(
        -decay_rate[None, :, None] * (tok_rows - 1.0 - position)[:, None, None]
    )
    own_state = jnp.einsum(
        "khd,khv->hdv",
        key_decayed,
        value_heads.astype(jnp.float32),
        precision=lax.Precision.HIGHEST,
    )
    block_decay = jnp.exp(-decay_rate * tok_rows)

    def link_states(earlier, later):
        return (earlier[0] * later[1][:, None, None] + later[0], earlier[1] * later[1])

    identity = (jnp.zeros_like(own_state), jnp.ones_like(block_decay))
    incoming, _ = entering((own_state, block_decay), "sp", link_states, identity)
    carried = jnp.einsum(
        "qhd,hdv->hqv", query_heads.astype(jnp.float32), incoming, precision=lax.Precision.HIGHEST
    )
    carried = carried * jnp.exp(-decay_col * (position + 1.0)[None, :, None])
    combined = intra_out + carried
    normed = combined * lax.rsqrt(jnp.mean(combined * combined, axis=-1, keepdims=True) + epsilon)
    normed = normed * state_gain.reshape(head_count, 1, DR)
    return normed.transpose(1, 0, 2).reshape(tok_rows, head_count * DR).astype(jnp.bfloat16)


def spread_body(
    tokens,
    norm_gain,
    query_weight,
    key_weight,
    value_weight,
    state_query,
    state_key,
    state_value,
    map_lambda,
    diff_gain,
    decay_rate,
    state_gain,
    out_weight,
):
    gathered = lax.all_gather(tokens[0], "tp", axis=1, tiled=True)
    tok_float = gathered.astype(jnp.float32)
    normed = tok_float * lax.rsqrt(
        jnp.mean(tok_float * tok_float, axis=-1, keepdims=True) + epsilon
    )
    normed = (normed * norm_gain).astype(jnp.bfloat16)
    pieces = (
        lax.all_gather(query_weight, "fs", axis=0, tiled=True),
        lax.all_gather(key_weight, "fs", axis=0, tiled=True),
        lax.all_gather(value_weight, "fs", axis=0, tiled=True),
        lax.all_gather(state_query, "fs", axis=0, tiled=True),
        lax.all_gather(state_key, "fs", axis=0, tiled=True),
        lax.all_gather(state_value, "fs", axis=0, tiled=True),
    )
    projected = tuple(
        (jnp.dot(normed, row_block, preferred_element_type=jnp.float32) for row_block in pieces)
    )
    att_query, att_keys, att_values, ret_query, ret_keys, ret_values = (
        member.astype(jnp.bfloat16) for member in projected
    )
    attended = attend(att_query, att_keys, att_values, map_lambda, diff_gain)
    retained = retain(ret_query, ret_keys, ret_values, decay_rate, state_gain)
    joined = jnp.concatenate([attended, retained], axis=1)
    diff_width = attended.shape[1]
    ret_width = retained.shape[1]
    tp_count = lax.axis_size("tp")
    tp_index = lax.axis_index("tp")
    own_rows = jnp.concatenate(
        [
            lax.dynamic_slice_in_dim(out_weight, tp_index * diff_width, diff_width, 0),
            lax.dynamic_slice_in_dim(
                out_weight, tp_count * diff_width + tp_index * ret_width, ret_width, 0
            ),
        ],
        axis=0,
    )
    output = lax.psum_scatter(
        jnp.dot(joined, own_rows, preferred_element_type=jnp.float32).astype(jnp.bfloat16),
        "tp",
        scatter_dimension=0,
        tiled=True,
    )
    return output[None]


def row_product(a, b):
    return lax.dot_general(a, b, (((1,), (1,)), ((), ())), preferred_element_type=jnp.float32)


def mixers_kernel(block, heads, proj, lam_ref, dgain_ref, rate_ref, sgain_ref, out):
    length = proj.shape[0]
    group = heads * DV
    place = lax.axis_index("sp")
    f32, bf16 = jnp.float32, jnp.bfloat16
    row = lax.broadcasted_iota(jnp.int32, (block, block), 0)
    col = lax.broadcasted_iota(jnp.int32, (block, block), 1)
    causal = col <= row
    lane = lax.broadcasted_iota(jnp.int32, (block, 2 * DK), 1)
    position = lax.broadcasted_iota(jnp.int32, (block, 1), 0).astype(f32)

    def part(kind, head, first, count):
        return proj[first : first + count, kind * group + head * DV : kind * group + head * DV + DV]

    for head in range(heads):
        spot = slice(head * DV, head * DV + DV)
        lam = lam_ref[place * heads + head]
        rate = rate_ref[place * heads + head]
        mine = pl.ds(pl.multiple_of((place * heads + head) * DV, DV), DV)
        gain = dgain_ref[:, mine] * branch_scale
        within = jnp.where(causal, jnp.exp(-rate * jnp.maximum(row - col, 0).astype(f32)), 0.0)
        query_decay = jnp.exp(-rate * (position + 1.0))
        key_decay = jnp.exp(-rate * (block - 1.0 - position))
        block_decay = jnp.exp(jnp.full((1, DR), -block, f32) * rate)
        state = jnp.zeros((DR, DR), f32)
        for turn in range(length // block):
            first = turn * block
            query = part(0, head, first, block) * jnp.asarray(DK ** (-0.5), bf16)
            averaged = []
            for which in range(2):
                own = jnp.where((lane >= DK) == bool(which), query, jnp.zeros_like(query))
                near = jnp.where(causal, row_product(own, part(1, head, first, block)), masked_score)
                peak = jnp.max(near, axis=1, keepdims=True)
                if first:
                    far = row_product(own, part(1, head, 0, first))
                    peak = jnp.maximum(peak, jnp.max(far, axis=1, keepdims=True))
                near = jnp.exp(near - peak)
                total = jnp.sum(near, axis=1, keepdims=True)
                summed = jnp.dot(near.astype(bf16), part(2, head, first, block), preferred_element_type=f32)
                if first:
                    far = jnp.exp(far - peak)
                    total = total + jnp.sum(far, axis=1, keepdims=True)
                    summed = summed + jnp.dot(
                        far.astype(bf16), part(2, head, 0, first), preferred_element_type=f32
                    )
                averaged.append(summed / total)
            differ = averaged[0] - lam * averaged[1]
            scaled = differ * lax.rsqrt(jnp.mean(differ * differ, axis=1, keepdims=True) + epsilon)
            out[first : first + block, spot] = (scaled * gain).astype(bf16)
            ret_query = part(3, head, first, block)
            ret_keys = part(4, head, first, block)
            ret_values = part(5, head, first, block)
            local = (row_product(ret_query, ret_keys) * within).astype(bf16)
            mixed = jnp.dot(local, ret_values, preferred_element_type=f32)
            if first:
                mixed = mixed + query_decay * jnp.dot(
                    ret_query, state.astype(bf16), preferred_element_type=f32
                )
            if first + block < length:
                decayed = (ret_keys.astype(f32) * key_decay).astype(bf16)
                state = state * block_decay + lax.dot_general(
                    decayed, ret_values, (((0,), (0,)), ((), ())), preferred_element_type=f32
                )
            scaled = mixed * lax.rsqrt(jnp.mean(mixed * mixed, axis=1, keepdims=True) + epsilon)
            out[first : first + block, group + head * DV : group + head * DV + DV] = (
                scaled * sgain_ref[:, mine]
            ).astype(bf16)


def mix(proj, block, heads, map_lambda, diff_gain, decay_rate, state_gain):
    length = proj.shape[0]
    vmem = pl.BlockSpec(memory_space=pltpu.VMEM)
    smem = pl.BlockSpec(memory_space=pltpu.SMEM)
    return pl.pallas_call(
        functools.partial(mixers_kernel, block, heads),
        out_shape=jax.ShapeDtypeStruct((length, 2 * heads * DV), jnp.bfloat16),
        in_specs=[vmem, smem, vmem, smem, vmem],
        out_specs=vmem,
        compiler_params=pltpu.CompilerParams(vmem_limit_bytes=65000 * 1024),
    )(
        proj,
        map_lambda,
        diff_gain[None],
        decay_rate,
        state_gain[None],
    )


MESH = pl.DeviceIdType.MESH


def greet(peers):
    barrier = pltpu.get_barrier_semaphore()
    count = 0
    for peer, present in peers:
        if present is None:
            pl.semaphore_signal(barrier, inc=1, device_id=peer, device_id_type=MESH)
            count = count + 1
        else:

            @pl.when(present)
            def _():
                pl.semaphore_signal(barrier, inc=1, device_id=peer, device_id_type=MESH)

            count = count + jnp.where(present, 1, 0)
    pl.semaphore_wait(barrier, count)


def project_kernel(
    line,
    tokens,
    gain,
    w0,
    w1,
    w2,
    w3,
    w4,
    w5,
    proj,
    seq,
    weight,
    local_sem,
    wsend,
    wrecv,
    lsend,
    lrecv,
    psend,
    precv,
):
    weights = (w0, w1, w2, w3, w4, w5)
    kinds = len(weights)
    half_kinds = kinds // 2
    z, f, c = lax.axis_index("sp"), lax.axis_index("fs"), lax.axis_index("tp")
    block, half = tokens.shape
    depth = w0.shape[0]
    width = weight.shape[1] // kinds
    near = ({"fs": f ^ 1}, {"fs": f ^ 2})
    whose = (f ^ 1, f ^ 2, f ^ 3)
    greet(
        [
            (near[0], None),
            (near[1], None),
            ({"tp": 1 - c}, None),
            ({"sp": jnp.minimum(z + 1, line - 1)}, z + 1 < line),
            ({"sp": jnp.maximum(z - 1, 0)}, z > 0),
        ]
    )

    def held(b, side):
        return seq.at[
            pl.ds(pl.multiple_of(b * block, block), block),
            pl.ds(pl.multiple_of(side * half, half), half),
        ]

    def stored(owner, kind):
        return weight.at[
            pl.ds(pl.multiple_of(owner * depth, depth), depth), kind * width : (kind + 1) * width
        ]

    def slot(e):
        if isinstance(e, int) and e == 0:
            return z
        up = (e - 1) % 2 == 0
        s = (e - 1) // 2
        return jnp.where(up, z - 1 - s, z + 1 + s)

    def along(e, b, source=None):
        up = (e - 1) % 2 == 0
        target = jnp.where(up, z + 1, z - 1)
        return pltpu.make_async_remote_copy(
            src_ref=held(b, c) if source is None else source,
            dst_ref=held(b, c),
            send_sem=lsend.at[e],
            recv_sem=lrecv.at[e],
            device_id={"sp": jnp.clip(target, 0, line - 1)},
            device_id_type=MESH,
        ), (target >= 0) & (target < line)

    def across(e, b, side, source=None):
        return pltpu.make_async_remote_copy(
            src_ref=held(b, side) if source is None else source,
            dst_ref=held(b, side),
            send_sem=psend.at[e],
            recv_sem=precv.at[e],
            device_id={"tp": 1 - c},
            device_id_type=MESH,
        )

    for e in (1, 2):
        copy, present = along(e, z, tokens)

        @pl.when(present)
        def _():
            copy.start()

    def own_columns(kind):
        return weights[kind].at[:, pl.ds(pl.multiple_of(z * width, width), width)]

    def spread(way, kind, source, owner, index):
        return pltpu.make_async_remote_copy(
            src_ref=source,
            dst_ref=stored(owner, kind),
            send_sem=wsend.at[way, index],
            recv_sem=wrecv.at[2 if index >= kinds else way, kind],
            device_id=near[way],
            device_id_type=MESH,
        )

    sends = []
    for turn in range(kinds):
        for way in range(2):
            kind = (turn + way * half_kinds) % kinds
            copy = spread(way, kind, own_columns(kind), f, kind)
            copy.start()
            sends.append(copy)
    across(0, z, c, tokens).start()
    locals_ = [pltpu.make_async_copy(tokens, held(z, c), local_sem.at[kinds])]
    for kind in range(kinds):
        locals_.append(pltpu.make_async_copy(own_columns(kind), stored(f, kind), local_sem.at[kind]))
    for copy in locals_:
        copy.start()

    def arrived(relation, kind):
        pltpu.make_async_remote_copy(
            src_ref=stored(whose[relation], kind),
            dst_ref=stored(whose[relation], kind),
            send_sem=wsend.at[0, kind],
            recv_sem=wrecv.at[relation, kind],
            device_id=near[0],
            device_id_type=MESH,
        ).wait_recv()

    for turn in range(half_kinds):
        for way in range(2):
            kind = turn + way * half_kinds
            arrived(way, kind)
            copy = spread(1 - way, kind, stored(whose[way], kind), whose[way], kinds + turn)
            copy.start()
            sends.append(copy)

    def take(s):
        for e in (1 + 2 * s, 2 + 2 * s):
            b = slot(e)

            @pl.when((b >= 0) & (b < line))
            def _():
                copy, _ = along(e, b)
                copy.wait_recv()
                if s + 1 < line - 1:
                    onward, present = along(e + 2, b)

                    @pl.when(present)
                    def _():
                        onward.start()

                across(e, b, c).start()

    def process(b):
        rows = pl.ds(pl.multiple_of(b * block, block), block)
        x = seq[rows, :].astype(jnp.float32)
        scaled = x * lax.rsqrt(jnp.mean(x * x, axis=1, keepdims=True) + epsilon)
        normed = (scaled * gain[...]).astype(jnp.bfloat16)
        proj[rows, :] = jnp.dot(normed, weight[...], preferred_element_type=jnp.float32).astype(
            jnp.bfloat16
        )

    def handle(e, carry):
        up = (e - 1) % 2 == 0
        s = (e - 1) // 2
        b = jnp.where(e == 0, z, jnp.where(up, z - 1 - s, z + 1 + s))

        @pl.when((b >= 0) & (b < line))
        def _():
            across(e, b, 1 - c).wait_recv()
            process(b)

        return carry

    for s in range(line - 2):
        take(s)
    for copy in locals_:
        copy.wait()
    for kind in range(kinds):
        for relation in range(3):
            if relation == 2 or not (relation * half_kinds <= kind < (relation + 1) * half_kinds):
                arrived(relation, kind)
    events = 2 * line - 1
    lax.fori_loop(0, events - 2, handle, 0)
    take(line - 2)
    lax.fori_loop(events - 2, events, handle, 0)

    for copy in sends:
        copy.wait_send()
    across(0, z, c, tokens).wait_send()
    for e in (1, 2):
        copy, present = along(e, z, tokens)

        @pl.when(present)
        def _():
            copy.wait_send()

    for s in range(line - 1):
        for e in (1 + 2 * s, 2 + 2 * s):
            b = slot(e)

            @pl.when((b >= 0) & (b < line))
            def _():
                across(e, b, c).wait_send()
                if s + 1 < line - 1:
                    onward, present = along(e + 2, b)

                    @pl.when(present)
                    def _():
                        onward.wait_send()


def gather_and_project(tokens, norm_gain, weights, line, width):
    block, half = tokens.shape
    kinds = len(weights)
    model = norm_gain.shape[0]
    anywhere = pl.BlockSpec(memory_space=pl.ANY)
    vmem = pl.BlockSpec(memory_space=pltpu.VMEM)
    events = 2 * line - 1
    dma = pltpu.SemaphoreType.DMA
    return pl.pallas_call(
        functools.partial(project_kernel, line),
        out_shape=jax.ShapeDtypeStruct((line * block, kinds * width), jnp.bfloat16),
        in_specs=[anywhere, vmem] + [anywhere] * kinds,
        out_specs=vmem,
        scratch_shapes=[
            pltpu.VMEM((line * block, model), jnp.bfloat16),
            pltpu.VMEM((model, kinds * width), jnp.bfloat16),
            dma((kinds + 1,)),
            dma((2, kinds + kinds // 2)),
            dma((3, kinds)),
            dma((events,)),
            dma((events,)),
            dma((events,)),
            dma((events,)),
        ],
        compiler_params=pltpu.CompilerParams(
            collective_id=0, has_side_effects=True, vmem_limit_bytes=65000 * 1024
        ),
    )(tokens, norm_gain[None], *weights)


def output_kernel(line, pair, mine, out_weight, result, joined, held, wsem, osem, send, recv):
    z, c = lax.axis_index("sp"), lax.axis_index("tp")
    count = line * pair
    me = z * pair + c
    rows = result.shape[0]
    width = mine.shape[1] // 2
    fetch = pltpu.make_async_copy(out_weight, held, wsem)
    fetch.start()
    peers = []
    for turn in range(1, count):
        other = (me + turn) % count
        peers.append((other, {"sp": other // pair, "tp": other % pair}))
    greet([(where, None) for _, where in peers])

    def place(source, which):
        first = which * (held.shape[0] // 2) + ((source % pair) * line + source // pair) * width
        return joined.at[:, pl.ds(pl.multiple_of(first, width), width)]

    def piece(target, which):
        return mine.at[
            pl.ds(pl.multiple_of(target * rows, rows), rows), which * width : (which + 1) * width
        ]

    def moved(turn, other, where, which, source):
        return pltpu.make_async_remote_copy(
            src_ref=piece(other, which),
            dst_ref=place(source, which),
            send_sem=send.at[turn, which],
            recv_sem=recv.at[turn, which],
            device_id=where,
            device_id_type=MESH,
        )

    for turn, (other, where) in enumerate(peers):
        for which in range(2):
            moved(turn, other, where, which, me).start()
    own = [pltpu.make_async_copy(piece(me, w), place(me, w), osem.at[w]) for w in range(2)]
    for copy in own:
        copy.start()
    for copy in own:
        copy.wait()
    fetch.wait()
    for turn, (other, where) in enumerate(peers):
        source = (me + count - turn - 1) % count
        for which in range(2):
            moved(turn, other, where, which, source).wait_recv()
    tile = 512

    def one(turn, carry):
        columns = pl.ds(pl.multiple_of(turn * tile, tile), tile)
        result[:, columns] = jnp.dot(
            joined[...], held[:, columns], preferred_element_type=jnp.float32
        ).astype(jnp.bfloat16)
        return carry

    lax.fori_loop(0, result.shape[1] // tile, one, 0)
    for turn, (other, where) in enumerate(peers):
        for which in range(2):
            moved(turn, other, where, which, me).wait_send()


def exchange_and_output(mine, out_weight, line, pair):
    count = line * pair
    rows = mine.shape[0] // count
    vmem = pl.BlockSpec(memory_space=pltpu.VMEM)
    dma = pltpu.SemaphoreType.DMA
    return pl.pallas_call(
        functools.partial(output_kernel, line, pair),
        out_shape=jax.ShapeDtypeStruct((rows, out_weight.shape[1]), jnp.bfloat16),
        in_specs=[vmem, pl.BlockSpec(memory_space=pl.ANY)],
        out_specs=vmem,
        scratch_shapes=[
            pltpu.VMEM((rows, out_weight.shape[0]), jnp.bfloat16),
            pltpu.VMEM(out_weight.shape, jnp.bfloat16),
            dma,
            dma((2,)),
            dma((count - 1, 2)),
            dma((count - 1, 2)),
        ],
        compiler_params=pltpu.CompilerParams(
            collective_id=1, has_side_effects=True, vmem_limit_bytes=65000 * 1024
        ),
    )(mine, out_weight)


def body(tokens, norm_gain, *rest):
    weights, (map_lambda, diff_gain, decay_rate, state_gain, out_weight) = rest[:6], rest[6:]
    line = lax.axis_size("sp")
    pair = lax.axis_size("tp")
    local = map_lambda.shape[0]
    if local % line or decay_rate.shape[0] != local or lax.axis_size("fs") != 4 or pair != 2:
        return spread_body(tokens, norm_gain, *rest)
    heads = local // line
    proj = gather_and_project(tokens[0], norm_gain, weights, line, heads * DV)
    mine = mix(proj, tokens.shape[1], heads, map_lambda, diff_gain, decay_rate, state_gain)
    return exchange_and_output(mine, out_weight, line, pair)[None]


def solution(mesh):
    placed = (
        P("fs", "sp", "tp"),
        P(),
        P("fs", "tp"),
        P("fs", "tp"),
        P("fs", "tp"),
        P("fs", "tp"),
        P("fs", "tp"),
        P("fs", "tp"),
        P("tp"),
        P("tp"),
        P("tp"),
        P("tp"),
        P(),
    )
    return jax.shard_map(
        body, mesh=mesh, in_specs=placed, out_specs=P("fs", ("sp", "tp"), None), check_vma=False
    )
```

profile of v0, /device:TPU:1, one launch (start us, length us, event | category | flops | bytes accessed | tf_op | source)
XLA Modules:
  0.0 70.6 jit_solution(2601591444420197141)
XLA Ops:
  0.0 46.3 %shard_map.127.proj = bf16[1024,768]{1,0:T(8,128)(2,1)} custom-call(bf16[256,1024]{1,0:T(8,128)(2,1)} %bitcast.6, f32[1,2048]{1,0:T(1,128)} %bitcast.7, bf16[512,512]{1,0:T(8,128)(2,1)} %w0.1, bf16[512,512]{1,0:T(8,128)(2,1)} %w1.1, bf16[512,512]{1,0:T(8,128)(2,1)} %w2.1, bf16[512,512]{1,0:T(8,128)(2,1)} %w3.1, bf16[512,512]{1,0:T(8,128)(2,1)} %w4.1, ...), custom_call_target="tpu_custom_call" | custom-call | tf_op jit(solution)/shard_map/pallas_call | solution.py:548
  46.3 6.1 %shard_map.128.mine = bf16[1024,256]{1,0:T(8,128)(2,1)} custom-call(bf16[1024,768]{1,0:T(8,128)(2,1)} %shard_map.127.proj, f32[4]{0:T(128)} %lam_ref.1, f32[1,512]{1,0:T(1,128)} %bitcast.8, f32[4]{0:T(128)} %rate_ref.1, f32[1,512]{1,0:T(1,128)} %bitcast.9), custom_call_target="tpu_custom_call" | custom-call | tf_op jit(solution)/shard_map/pallas_call | solution.py:297
  52.4 16.3 %shard_map.129 = bf16[128,2048]{1,0:T(8,128)(2,1)} custom-call(bf16[1024,256]{1,0:T(8,128)(2,1)} %shard_map.128.mine, bf16[2048,2048]{1,0:T(8,128)(2,1)} %out_weight.1), custom_call_target="tpu_custom_call" | custom-call | tf_op jit(solution)/shard_map/pallas_call | solution.py:636
  68.7 1.9 %copy.15 = bf16[1,128,2048]{2,1,0:T(8,128)(2,1)} copy(bf16[1,128,2048]{2,1,0:T(8,128)(2,1)} %bitcast.5) | data formatting | bytes 1048576
where the time goes:
time: 71.6 us; the launch traced here: 70.6 us
  Pallas kernels  68.7 us (96%)
  local copies, waits for them, and re-layouts  1.88 us (3%)
    pallas_call x1, Pallas kernels, gather_and_project(): pl.pallas_call(functools.partial(project_kernel, line), out_shape=jax.Sha...  46.3 us
    pallas_call x1, Pallas kernels, exchange_and_output(): pl.pallas_call(functools.partial(output_kernel, line, pair), out_shape=ja...  16.3 us
    pallas_call x1, Pallas kernels, mix(): pl.pallas_call(functools.partial(mixers_kernel, block, heads), out_shape=...  6.1 us
    unnamed x1, local copies, waits for them, and re-layouts  1.88 us

commit v1 on v0

v1 whole, which is shorter than its diff:
```python
import functools

import jax
import jax.numpy as jnp
from jax import lax
from jax.experimental import pallas as pl
from jax.experimental.pallas import tpu as pltpu
from jax.sharding import PartitionSpec as P

DK = 64
DV = 128
DR = 128


epsilon = 1e-05
branch_scale = 0.8
masked_score = -1e30


def from_behind(x, axis, by):
    size = lax.axis_size(axis)
    pairs = [(i, i + by) for i in range(size) if 0 <= i + by < size]
    return lax.ppermute(x, axis, pairs)


def entering(x, axis, join, neutral):
    place = lax.axis_index(axis)
    gathered = jax.tree.map(
        lambda a, kind: lax.all_gather(a.astype(kind), axis), x, (jnp.bfloat16, jnp.bfloat16)
    )
    state = jax.tree.map(lambda a, e: jnp.zeros_like(a) + jnp.asarray(e, a.dtype), x, neutral)

    def one(turn, state):
        return join(
            state,
            jax.tree.map(
                lambda a, own: lax.dynamic_index_in_dim(a, turn, 0, False).astype(own.dtype),
                gathered,
                x,
            ),
        )

    return lax.fori_loop(0, place, one, state)


def attend(att_query, att_keys, att_values, map_lambda, diff_gain):
    tok_rows = att_query.shape[0]
    head_count = map_lambda.shape[0]
    key_width = att_keys.shape[1]
    query_heads = att_query.reshape(tok_rows, head_count, 2, DK)
    sp_index = lax.axis_index("sp")
    query_place = sp_index * tok_rows + jnp.arange(tok_rows)
    score_scale = DK ** (-0.5)

    def absorb_block(running, inputs):
        key_block, key_place = inputs
        key_heads = key_block[:, :key_width].reshape(tok_rows, head_count, 2, DK)
        value_heads = key_block[:, key_width:].reshape(tok_rows, head_count, DV)
        scores = (
            jnp.einsum(
                "qhmd,khmd->mhqk", query_heads, key_heads, preferred_element_type=jnp.float32
            )
            * score_scale
        )
        causal = key_place[None, :] <= query_place[:, None]
        row_peak, totals, summed = running
        new_peak = jnp.maximum(row_peak, jnp.max(jnp.where(causal, scores, masked_score), axis=-1))
        weights = jnp.where(causal, jnp.exp(scores - new_peak[..., None]), 0.0)
        factor = jnp.exp(row_peak - new_peak)
        totals = totals * factor + jnp.sum(weights, axis=-1)
        summed = summed * factor[..., None] + jnp.einsum(
            "mhqk,khv->mhqv",
            weights.astype(jnp.bfloat16),
            value_heads,
            preferred_element_type=jnp.float32,
        )
        return ((new_peak, totals, summed), None)

    def absorb(running, pieces, first_row):
        piece_rows = pieces.shape[0]
        stacked = pieces.reshape(piece_rows // tok_rows, tok_rows, pieces.shape[1])
        places = (first_row + jnp.arange(piece_rows)).reshape(piece_rows // tok_rows, tok_rows)
        return lax.scan(absorb_block, running, (stacked, places))[0]

    starting = (
        jnp.full((2, head_count, tok_rows), masked_score, jnp.float32),
        jnp.zeros((2, head_count, tok_rows), jnp.float32),
        jnp.zeros((2, head_count, tok_rows, DV), jnp.float32),
    )
    joined_kv = jnp.concatenate([att_keys, att_values], axis=1)
    first_state = absorb(starting, joined_kv, sp_index * tok_rows)

    def relay_step(step_index, relay_state):
        running, moving = relay_state
        moving = from_behind(moving, "sp", 1)
        first_row = (sp_index - step_index) * tok_rows
        running = lax.cond(
            first_row >= 0,
            lambda holding: absorb(holding, moving, first_row),
            lambda holding: holding,
            running,
        )
        return (running, moving)

    running, _ = lax.fori_loop(1, lax.axis_size("sp"), relay_step, (first_state, joined_kv))
    row_peak, totals, summed = running
    averaged = summed / totals[..., None]
    differ = averaged[0] - map_lambda[:, None, None] * averaged[1]
    normed = differ * lax.rsqrt(jnp.mean(differ * differ, axis=-1, keepdims=True) + epsilon)
    normed = normed * diff_gain.reshape(head_count, 1, DV) * branch_scale
    return normed.transpose(1, 0, 2).reshape(tok_rows, head_count * DV).astype(jnp.bfloat16)


def retain(ret_query, ret_keys, ret_values, decay_rate, state_gain):
    tok_rows = ret_query.shape[0]
    head_count = decay_rate.shape[0]
    query_heads = ret_query.reshape(tok_rows, head_count, DR)
    key_heads = ret_keys.reshape(tok_rows, head_count, DR)
    value_heads = ret_values.reshape(tok_rows, head_count, DR)
    position = jnp.arange(tok_rows).astype(jnp.float32)
    distance = position[:, None] - position[None, :]
    decay_col = decay_rate[:, None, None]
    within = jnp.where(distance >= 0, jnp.exp(-decay_col * jnp.maximum(distance, 0.0)), 0.0)
    local_scores = (
        jnp.einsum("qhd,khd->hqk", query_heads, key_heads, preferred_element_type=jnp.float32)
        * within
    )
    intra_out = jnp.einsum(
        "hqk,khv->hqv",
        local_scores.astype(jnp.bfloat16),
        value_heads,
        preferred_element_type=jnp.float32,
    )
    key_decayed = key_heads.astype(jnp.float32) * jnp.exp(
        -decay_rate[None, :, None] * (tok_rows - 1.0 - position)[:, None, None]
    )
    own_state = jnp.einsum(
        "khd,khv->hdv",
        key_decayed,
        value_heads.astype(jnp.float32),
        precision=lax.Precision.HIGHEST,
    )
    block_decay = jnp.exp(-decay_rate * tok_rows)

    def link_states(earlier, later):
        return (earlier[0] * later[1][:, None, None] + later[0], earlier[1] * later[1])

    identity = (jnp.zeros_like(own_state), jnp.ones_like(block_decay))
    incoming, _ = entering((own_state, block_decay), "sp", link_states, identity)
    carried = jnp.einsum(
        "qhd,hdv->hqv", query_heads.astype(jnp.float32), incoming, precision=lax.Precision.HIGHEST
    )
    carried = carried * jnp.exp(-decay_col * (position + 1.0)[None, :, None])
    combined = intra_out + carried
    normed = combined * lax.rsqrt(jnp.mean(combined * combined, axis=-1, keepdims=True) + epsilon)
    normed = normed * state_gain.reshape(head_count, 1, DR)
    return normed.transpose(1, 0, 2).reshape(tok_rows, head_count * DR).astype(jnp.bfloat16)


def spread_body(
    tokens,
    norm_gain,
    query_weight,
    key_weight,
    value_weight,
    state_query,
    state_key,
    state_value,
    map_lambda,
    diff_gain,
    decay_rate,
    state_gain,
    out_weight,
):
    gathered = lax.all_gather(tokens[0], "tp", axis=1, tiled=True)
    tok_float = gathered.astype(jnp.float32)
    normed = tok_float * lax.rsqrt(
        jnp.mean(tok_float * tok_float, axis=-1, keepdims=True) + epsilon
    )
    normed = (normed * norm_gain).astype(jnp.bfloat16)
    pieces = (
        lax.all_gather(query_weight, "fs", axis=0, tiled=True),
        lax.all_gather(key_weight, "fs", axis=0, tiled=True),
        lax.all_gather(value_weight, "fs", axis=0, tiled=True),
        lax.all_gather(state_query, "fs", axis=0, tiled=True),
        lax.all_gather(state_key, "fs", axis=0, tiled=True),
        lax.all_gather(state_value, "fs", axis=0, tiled=True),
    )
    projected = tuple(
        (jnp.dot(normed, row_block, preferred_element_type=jnp.float32) for row_block in pieces)
    )
    att_query, att_keys, att_values, ret_query, ret_keys, ret_values = (
        member.astype(jnp.bfloat16) for member in projected
    )
    attended = attend(att_query, att_keys, att_values, map_lambda, diff_gain)
    retained = retain(ret_query, ret_keys, ret_values, decay_rate, state_gain)
    joined = jnp.concatenate([attended, retained], axis=1)
    diff_width = attended.shape[1]
    ret_width = retained.shape[1]
    tp_count = lax.axis_size("tp")
    tp_index = lax.axis_index("tp")
    own_rows = jnp.concatenate(
        [
            lax.dynamic_slice_in_dim(out_weight, tp_index * diff_width, diff_width, 0),
            lax.dynamic_slice_in_dim(
                out_weight, tp_count * diff_width + tp_index * ret_width, ret_width, 0
            ),
        ],
        axis=0,
    )
    output = lax.psum_scatter(
        jnp.dot(joined, own_rows, preferred_element_type=jnp.float32).astype(jnp.bfloat16),
        "tp",
        scatter_dimension=0,
        tiled=True,
    )
    return output[None]


def row_product(a, b):
    return lax.dot_general(a, b, (((1,), (1,)), ((), ())), preferred_element_type=jnp.float32)


MESH = pl.DeviceIdType.MESH


def greet(peers):
    barrier = pltpu.get_barrier_semaphore()
    count = 0
    for peer, present in peers:
        if present is None:
            pl.semaphore_signal(barrier, inc=1, device_id=peer, device_id_type=MESH)
            count = count + 1
        else:

            @pl.when(present)
            def _():
                pl.semaphore_signal(barrier, inc=1, device_id=peer, device_id_type=MESH)

            count = count + jnp.where(present, 1, 0)
    pl.semaphore_wait(barrier, count)


def layer_kernel(
    line,
    parts,
    tokens,
    gain,
    w0,
    w1,
    w2,
    w3,
    w4,
    w5,
    lam_ref,
    dgain_ref,
    rate_ref,
    sgain_ref,
    out_weight,
    result,
    seq,
    weight,
    proj,
    mine,
    joined,
    held,
    state,
    total,
    local_sem,
    held_sem,
    wsend,
    wrecv,
    lsend,
    lrecv,
    psend,
    precv,
    osend,
    orecv,
):
    f32, bf16 = jnp.float32, jnp.bfloat16
    weights = (w0, w1, w2, w3, w4, w5)
    kinds = len(weights)
    half_kinds = kinds // 2
    z, f, c = lax.axis_index("sp"), lax.axis_index("fs"), lax.axis_index("tp")
    block, half = tokens.shape
    piece = block // parts
    depth = w0.shape[0]
    width = weight.shape[1] // kinds
    rows_out = result.shape[0]
    me = c * line + z
    near = ({"fs": f ^ 1}, {"fs": f ^ 2})
    whose = (f ^ 1, f ^ 2, f ^ 3)
    greet(
        [
            (near[0], None),
            (near[1], None),
            ({"tp": 1 - c}, None),
            ({"sp": jnp.minimum(z + 1, line - 1)}, z + 1 < line),
            ({"sp": jnp.maximum(z - 1, 0)}, z > 0),
        ]
    )

    def held_at(b, side, q):
        return seq.at[
            pl.ds(pl.multiple_of(b * block + q * piece, piece), piece),
            pl.ds(pl.multiple_of(side * half, half), half),
        ]

    def own_tokens(q):
        return tokens.at[q * piece : (q + 1) * piece, :]

    def stored(owner, kind):
        return weight.at[
            pl.ds(pl.multiple_of(owner * depth, depth), depth), kind * width : (kind + 1) * width
        ]

    def slot(e):
        up = (e - 1) % 2 == 0
        s = (e - 1) // 2
        return z - 1 - s if up else z + 1 + s

    def along(e, b, q, source=None):
        target = z + 1 if (e - 1) % 2 == 0 else z - 1
        return pltpu.make_async_remote_copy(
            src_ref=held_at(b, c, q) if source is None else source,
            dst_ref=held_at(b, c, q),
            send_sem=lsend.at[e, q],
            recv_sem=lrecv.at[e, q],
            device_id={"sp": jnp.clip(target, 0, line - 1)},
            device_id_type=MESH,
        ), (target >= 0) & (target < line)

    def across(e, b, side, q, source=None):
        return pltpu.make_async_remote_copy(
            src_ref=held_at(b, side, q) if source is None else source,
            dst_ref=held_at(b, side, q),
            send_sem=psend.at[e, q],
            recv_sem=precv.at[e, q],
            device_id={"tp": 1 - c},
            device_id_type=MESH,
        )

    def own_columns(kind):
        return weights[kind].at[:, pl.ds(pl.multiple_of(z * width, width), width)]

    def spread(way, kind, source, owner, index):
        return pltpu.make_async_remote_copy(
            src_ref=source,
            dst_ref=stored(owner, kind),
            send_sem=wsend.at[way, index],
            recv_sem=wrecv.at[2 if index >= kinds else way, kind],
            device_id=near[way],
            device_id_type=MESH,
        )

    def arrived(relation, kind):
        pltpu.make_async_remote_copy(
            src_ref=stored(whose[relation], kind),
            dst_ref=stored(whose[relation], kind),
            send_sem=wsend.at[0, kind],
            recv_sem=wrecv.at[relation, kind],
            device_id=near[0],
            device_id_type=MESH,
        ).wait_recv()

    for q in range(parts):
        for e in (1, 2):
            copy, present = along(e, z, q, own_tokens(q))

            @pl.when(present)
            def _():
                copy.start()

    sends = []
    for turn in range(kinds):
        for way in range(2):
            kind = (turn + way * half_kinds) % kinds
            copy = spread(way, kind, own_columns(kind), f, kind)
            copy.start()
            sends.append(copy)
    locals_ = []
    for q in range(parts):
        across(0, z, c, q, own_tokens(q)).start()
        locals_.append(
            pltpu.make_async_copy(own_tokens(q), held_at(z, c, q), local_sem.at[kinds + q])
        )
    for kind in range(kinds):
        locals_.append(pltpu.make_async_copy(own_columns(kind), stored(f, kind), local_sem.at[kind]))
    for copy in locals_:
        copy.start()

    def relay(turn):
        for way in range(2):
            kind = turn + way * half_kinds
            arrived(way, kind)
            copy = spread(1 - way, kind, stored(whose[way], kind), whose[way], kinds + turn)
            copy.start()
            sends.append(copy)

    def take(s, q):
        for e in (1 + 2 * s, 2 + 2 * s):
            b = slot(e)

            @pl.when((b >= 0) & (b < line))
            def _():
                copy, _ = along(e, b, q)
                copy.wait_recv()
                if s + 1 < line - 1:
                    onward, present = along(e + 2, b, q)

                    @pl.when(present)
                    def _():
                        onward.start()

                across(e, b, c, q).start()

    def fetch(index):
        source = index // 2
        kind = index % 2
        first = kind * (out_weight.shape[0] // 2) + source * width
        return pltpu.make_async_copy(
            out_weight.at[first : first + width, :],
            held.at[source, kind * width : (kind + 1) * width, :],
            held_sem.at[index],
        )

    fetches = [fetch(index) for index in range(2 * joined.shape[0])]
    early = [(s, q) for s in range(line - 2) for q in range(parts)]
    for turn in range(half_kinds):
        relay(turn)
        if turn == 0:
            for copy in fetches:
                copy.start()
        elif early:
            take(*early.pop(0))
    for s, q in early:
        take(s, q)
    for copy in locals_:
        copy.wait()
    for kind in range(kinds):
        for relation in range(3):
            if relation == 2 or not (relation * half_kinds <= kind < (relation + 1) * half_kinds):
                arrived(relation, kind)

    def process(b):
        rows = pl.ds(pl.multiple_of(b * block, block), block)
        x = seq[rows, :].astype(f32)
        scaled = x * lax.rsqrt(jnp.mean(x * x, axis=1, keepdims=True) + epsilon)
        normed = (scaled * gain[...]).astype(bf16)
        proj[rows, :] = jnp.dot(normed, weight[...], preferred_element_type=f32).astype(bf16)

    def handle(e, carry):
        up = (e - 1) % 2 == 0
        s = (e - 1) // 2
        b = jnp.where(e == 0, z, jnp.where(up, z - 1 - s, z + 1 + s))

        @pl.when((b >= 0) & (b < line))
        def _():
            for q in range(parts):
                across(e, b, 1 - c, q).wait_recv()
            process(b)

        return carry

    row = lax.broadcasted_iota(jnp.int32, (block, block), 0)
    col = lax.broadcasted_iota(jnp.int32, (block, block), 1)
    lane = lax.broadcasted_iota(jnp.int32, (block, 2 * DK), 1)
    position = lax.broadcasted_iota(jnp.int32, (block, 1), 0).astype(f32)
    own_lanes = pl.ds(pl.multiple_of(z * DV, DV), DV)

    def part(kind, first, count):
        return proj[first : first + count, kind * DV : kind * DV + DV]

    def mix(b):
        first = b * block
        causal = col <= row
        lam = lam_ref[z]
        rate = rate_ref[z]
        query = part(0, first, block) * jnp.asarray(DK ** (-0.5), bf16)
        averaged = []
        for which in range(2):
            own = jnp.where((lane >= DK) == bool(which), query, jnp.zeros_like(query))
            near_scores = jnp.where(causal, row_product(own, part(1, first, block)), masked_score)
            peak = jnp.max(near_scores, axis=1, keepdims=True)
            if first:
                far = row_product(own, part(1, 0, first))
                peak = jnp.maximum(peak, jnp.max(far, axis=1, keepdims=True))
            near_scores = jnp.exp(near_scores - peak)
            count = jnp.sum(near_scores, axis=1, keepdims=True)
            summed = jnp.dot(
                near_scores.astype(bf16), part(2, first, block), preferred_element_type=f32
            )
            if first:
                far = jnp.exp(far - peak)
                count = count + jnp.sum(far, axis=1, keepdims=True)
                summed = summed + jnp.dot(
                    far.astype(bf16), part(2, 0, first), preferred_element_type=f32
                )
            averaged.append(summed / count)
        differ = averaged[0] - lam * averaged[1]
        scaled = differ * lax.rsqrt(jnp.mean(differ * differ, axis=1, keepdims=True) + epsilon)
        mine[first : first + block, :DV] = (
            scaled * (dgain_ref[:, own_lanes] * branch_scale)
        ).astype(bf16)
        ret_query = part(3, first, block)
        ret_keys = part(4, first, block)
        ret_values = part(5, first, block)
        within = jnp.where(causal, jnp.exp(-rate * jnp.maximum(row - col, 0).astype(f32)), 0.0)
        local = (row_product(ret_query, ret_keys) * within).astype(bf16)
        mixed = jnp.dot(local, ret_values, preferred_element_type=f32)
        if first:
            mixed = mixed + jnp.exp(-rate * (position + 1.0)) * jnp.dot(
                ret_query, state[...].astype(bf16), preferred_element_type=f32
            )
        if b + 1 < line:
            decayed = (ret_keys.astype(f32) * jnp.exp(-rate * (block - 1.0 - position))).astype(bf16)
            update = lax.dot_general(
                decayed, ret_values, (((0,), (0,)), ((), ())), preferred_element_type=f32
            )
            if first:
                update = state[...] * jnp.exp(jnp.full((1, DR), -block, f32) * rate) + update
            state[...] = update
        scaled = mixed * lax.rsqrt(jnp.mean(mixed * mixed, axis=1, keepdims=True) + epsilon)
        mine[first : first + block, DV:] = (scaled * sgain_ref[:, own_lanes]).astype(bf16)

    def mine_rows(b, side):
        return mine.at[pl.ds(pl.multiple_of(b * block + side * rows_out, rows_out), rows_out), :]

    def deliver(b, turn):
        side = c if turn == 0 else 1 - c
        return pltpu.make_async_remote_copy(
            src_ref=mine_rows(b, side),
            dst_ref=joined.at[me],
            send_sem=osend.at[b, turn],
            recv_sem=orecv.at[me],
            device_id={"sp": b, "tp": side},
            device_id_type=MESH,
        )

    def give(b):
        deliver(b, 1).start()

        @pl.when(z != b)
        def _():
            deliver(b, 0).start()

        @pl.when(z == b)
        def _():
            joined[me] = mine_rows(b, c)[...]

    last = 2 * line - 3
    lax.fori_loop(0, last, handle, 0)

    def phase(t, carry):
        @pl.when(t == 1)
        def _():
            for q in range(parts):
                take(line - 2, q)
            lax.fori_loop(last, last + 2, handle, 0)

        for b in range(line):
            late = z == line - 1
            if b == line - 1:
                late = late | (z == 0)

            @pl.when(late == (t == 1))
            def _():
                mix(b)
                give(b)

        return carry

    lax.fori_loop(0, 2, phase, 0)

    for copy in fetches:
        copy.wait()
    order = [s for s in range(1, line - 1)] + [0, line - 1]
    for index, source in enumerate(order):
        for turn in range(2):
            side = c if turn == 0 else 1 - c
            where = side * line + source

            @pl.when(where != me)
            def _():
                pltpu.make_async_remote_copy(
                    src_ref=joined.at[where],
                    dst_ref=joined.at[where],
                    send_sem=osend.at[0, 0],
                    recv_sem=orecv.at[where],
                    device_id={"tp": 1 - c},
                    device_id_type=MESH,
                ).wait_recv()

            product = jnp.dot(joined[where], held[where], preferred_element_type=f32)
            if index == 0 and turn == 0:
                total[...] = product
            elif index < line - 1 or turn == 0:
                total[...] += product
            else:
                result[...] = (total[...] + product).astype(bf16)

    for copy in sends:
        copy.wait_send()
    for q in range(parts):
        across(0, z, c, q, own_tokens(q)).wait_send()
        for e in (1, 2):
            copy, present = along(e, z, q, own_tokens(q))

            @pl.when(present)
            def _():
                copy.wait_send()

        for s in range(line - 1):
            for e in (1 + 2 * s, 2 + 2 * s):
                b = slot(e)

                @pl.when((b >= 0) & (b < line))
                def _():
                    across(e, b, c, q).wait_send()
                    if s + 1 < line - 1:
                        onward, present = along(e + 2, b, q)

                        @pl.when(present)
                        def _():
                            onward.wait_send()

    for b in range(line):
        deliver(b, 1).wait_send()

        @pl.when(z != b)
        def _():
            deliver(b, 0).wait_send()


def whole_layer(tokens, norm_gain, weights, map_lambda, diff_gain, decay_rate, state_gain, out_weight, line, pair):
    block, half = tokens.shape
    kinds = len(weights)
    model = norm_gain.shape[0]
    parts = 2
    rows = block // pair
    count = line * pair
    anywhere = pl.BlockSpec(memory_space=pl.ANY)
    vmem = pl.BlockSpec(memory_space=pltpu.VMEM)
    smem = pl.BlockSpec(memory_space=pltpu.SMEM)
    events = 2 * line - 1
    dma = pltpu.SemaphoreType.DMA
    bf16 = jnp.bfloat16
    return pl.pallas_call(
        functools.partial(layer_kernel, line, parts),
        out_shape=jax.ShapeDtypeStruct((rows, out_weight.shape[1]), bf16),
        in_specs=[anywhere, vmem] + [anywhere] * kinds + [smem, vmem, smem, vmem, anywhere],
        out_specs=vmem,
        scratch_shapes=[
            pltpu.VMEM((line * block, model), bf16),
            pltpu.VMEM((model, kinds * DV), bf16),
            pltpu.VMEM((line * block, kinds * DV), bf16),
            pltpu.VMEM((line * block, 2 * DV), bf16),
            pltpu.VMEM((count, rows, 2 * DV), bf16),
            pltpu.VMEM((count, 2 * DV, out_weight.shape[1]), bf16),
            pltpu.VMEM((DR, DR), jnp.float32),
            pltpu.VMEM((rows, out_weight.shape[1]), jnp.float32),
            dma((kinds + parts,)),
            dma((2 * count,)),
            dma((2, kinds + kinds // 2)),
            dma((3, kinds)),
            dma((events, parts)),
            dma((events, parts)),
            dma((events, parts)),
            dma((events, parts)),
            dma((line, pair)),
            dma((count,)),
        ],
        compiler_params=pltpu.CompilerParams(
            collective_id=0, has_side_effects=True, vmem_limit_bytes=65000 * 1024
        ),
    )(
        tokens,
        norm_gain[None],
        *weights,
        map_lambda,
        diff_gain[None],
        decay_rate,
        state_gain[None],
        out_weight,
    )


def body(tokens, norm_gain, *rest):
    weights, (map_lambda, diff_gain, decay_rate, state_gain, out_weight) = rest[:6], rest[6:]
    line = lax.axis_size("sp")
    pair = lax.axis_size("tp")
    local = map_lambda.shape[0]
    if local != line or decay_rate.shape[0] != local or lax.axis_size("fs") != 4 or pair != 2:
        return spread_body(tokens, norm_gain, *rest)
    return whole_layer(
        tokens[0],
        norm_gain,
        weights,
        map_lambda,
        diff_gain,
        decay_rate,
        state_gain,
        out_weight,
        line,
        pair,
    )[None]


def solution(mesh):
    placed = (
        P("fs", "sp", "tp"),
        P(),
        P("fs", "tp"),
        P("fs", "tp"),
        P("fs", "tp"),
        P("fs", "tp"),
        P("fs", "tp"),
        P("fs", "tp"),
        P("tp"),
        P("tp"),
        P("tp"),
        P("tp"),
        P(),
    )
    return jax.shard_map(
        body, mesh=mesh, in_specs=placed, out_specs=P("fs", ("sp", "tp"), None), check_vma=False
    )
```

time: 71.6 us -> 55.5 us (0.78)
  the two profiles are of different devices: /device:TPU:1 before, /device:TPU:17 now
where the time goes in v1:
time: 55.5 us; the launch traced here: 55.3 us
  Pallas kernels  53.4 us (96%)
  local copies, waits for them, and re-layouts  1.88 us (3%)
    pallas_call x1, Pallas kernels, whole_layer(): pl.pallas_call(functools.partial(layer_kernel, line, parts), out_shape=ja...  53.4 us
    unnamed x1, local copies, waits for them, and re-layouts  1.88 us

profile of v1, /device:TPU:17, one launch (start us, length us, event | category | flops | bytes accessed | tf_op | source)
XLA Modules:
  0.0 55.3 jit_solution(13029120592327176850)
XLA Ops:
  0.0 53.4 %shard_map.127 = bf16[128,2048]{1,0:T(8,128)(2,1)} custom-call(bf16[256,1024]{1,0:T(8,128)(2,1)} %bitcast.6, f32[1,2048]{1,0:T(1,128)} %bitcast.7, bf16[512,512]{1,0:T(8,128)(2,1)} %w0.1, bf16[512,512]{1,0:T(8,128)(2,1)} %w1.1, bf16[512,512]{1,0:T(8,128)(2,1)} %w2.1, bf16[512,512]{1,0:T(8,128)(2,1)} %w3.1, bf16[512,512]{1,0:T(8,128)(2,1)} %w4.1, ...), custom_call_target="tpu_custom_call" | custom-call | tf_op jit(solution)/shard_map/pallas_call | solution.py:648
  53.4 1.9 %copy.15 = bf16[1,128,2048]{2,1,0:T(8,128)(2,1)} copy(bf16[1,128,2048]{2,1,0:T(8,128)(2,1)} %bitcast.5) | data formatting | bytes 1048576

commit v2 on v1

--- a/solution.py
+++ b/solution.py
@@ -245,20 +245,24 @@
     line,
     parts,
     tokens,
-    gain,
+    gain_in,
     w0,
     w1,
     w2,
     w3,
     w4,
     w5,
-    lam_ref,
-    dgain_ref,
-    rate_ref,
-    sgain_ref,
+    lam_in,
+    dgain_in,
+    rate_in,
+    sgain_in,
     out_weight,
     result,
+    gains,
+    lam_ref,
+    rate_ref,
     seq,
+    normal,
     weight,
     proj,
     mine,
@@ -281,12 +285,15 @@
     weights = (w0, w1, w2, w3, w4, w5)
     kinds = len(weights)
     half_kinds = kinds // 2
+    early_parts = parts // 2
+    events = 2 * line - 1
     z, f, c = lax.axis_index("sp"), lax.axis_index("fs"), lax.axis_index("tp")
     block, half = tokens.shape
     piece = block // parts
     depth = w0.shape[0]
     width = weight.shape[1] // kinds
     rows_out = result.shape[0]
+    model = seq.shape[1]
     me = c * line + z
     near = ({"fs": f ^ 1}, {"fs": f ^ 2})
     whose = (f ^ 1, f ^ 2, f ^ 3)
@@ -306,12 +313,21 @@
             pl.ds(pl.multiple_of(side * half, half), half),
         ]
 
+    def whole(b, side):
+        return seq.at[
+            pl.ds(pl.multiple_of(b * block, block), block),
+            pl.ds(pl.multiple_of(side * half, half), half),
+        ]
+
     def own_tokens(q):
         return tokens.at[q * piece : (q + 1) * piece, :]
 
+    def column(kind):
+        return (2 * (kind % half_kinds) + kind // half_kinds) * width
+
     def stored(owner, kind):
         return weight.at[
-            pl.ds(pl.multiple_of(owner * depth, depth), depth), kind * width : (kind + 1) * width
+            pl.ds(pl.multiple_of(owner * depth, depth), depth), column(kind) : column(kind) + width
         ]
 
     def slot(e):
@@ -324,7 +340,7 @@
         return pltpu.make_async_remote_copy(
             src_ref=held_at(b, c, q) if source is None else source,
             dst_ref=held_at(b, c, q),
-            send_sem=lsend.at[e, q],
+            send_sem=lsend.at[e],
             recv_sem=lrecv.at[e, q],
             device_id={"sp": jnp.clip(target, 0, line - 1)},
             device_id_type=MESH,
@@ -334,21 +350,44 @@
         return pltpu.make_async_remote_copy(
             src_ref=held_at(b, side, q) if source is None else source,
             dst_ref=held_at(b, side, q),
-            send_sem=psend.at[e, q],
-            recv_sem=precv.at[e, q],
+            send_sem=psend.at[e],
+            recv_sem=precv.at[e],
             device_id={"tp": 1 - c},
             device_id_type=MESH,
         )
 
+    def all_along(e):
+        return pltpu.make_async_remote_copy(
+            src_ref=tokens,
+            dst_ref=whole(z, c),
+            send_sem=lsend.at[e],
+            recv_sem=lrecv.at[e, 0],
+            device_id={"sp": z ^ 1},
+            device_id_type=MESH,
+        )
+
+    def all_across(e, b):
+        return pltpu.make_async_remote_copy(
+            src_ref=whole(b, 1 - c),
+            dst_ref=whole(b, 1 - c),
+            send_sem=psend.at[e],
+            recv_sem=precv.at[e],
+            device_id={"tp": 1 - c},
+            device_id_type=MESH,
+        )
+
     def own_columns(kind):
         return weights[kind].at[:, pl.ds(pl.multiple_of(z * width, width), width)]
+
+    def arrival(relation, kind):
+        return kind if relation == kind // half_kinds else kinds + kind % half_kinds
 
     def spread(way, kind, source, owner, index):
         return pltpu.make_async_remote_copy(
             src_ref=source,
             dst_ref=stored(owner, kind),
-            send_sem=wsend.at[way, index],
-            recv_sem=wrecv.at[2 if index >= kinds else way, kind],
+            send_sem=wsend,
+            recv_sem=wrecv.at[arrival(2 if index >= kinds else way, kind)],
             device_id=near[way],
             device_id_type=MESH,
         )
@@ -357,35 +396,44 @@
         pltpu.make_async_remote_copy(
             src_ref=stored(whose[relation], kind),
             dst_ref=stored(whose[relation], kind),
-            send_sem=wsend.at[0, kind],
-            recv_sem=wrecv.at[relation, kind],
+            send_sem=wsend,
+            recv_sem=wrecv.at[arrival(relation, kind)],
             device_id=near[0],
             device_id_type=MESH,
         ).wait_recv()
 
+    def push(e, q, when=True):
+        copy, present = along(e, z, q, own_tokens(q))
+
+        @pl.when(present & when)
+        def _():
+            copy.start()
+
+    def scatter(pair):
+        for kind in (pair, pair + half_kinds):
+            for way in range(2):
+                spread(way, kind, own_columns(kind), f, kind).start()
+
     for q in range(parts):
-        for e in (1, 2):
-            copy, present = along(e, z, q, own_tokens(q))
-
-            @pl.when(present)
-            def _():
-                copy.start()
-
-    sends = []
-    for turn in range(kinds):
-        for way in range(2):
-            kind = (turn + way * half_kinds) % kinds
-            copy = spread(way, kind, own_columns(kind), f, kind)
-            copy.start()
-            sends.append(copy)
+        push(1, q, z >= 0 if q < early_parts else z == 0)
+        push(2, q)
+    scatter(0)
     locals_ = []
     for q in range(parts):
         across(0, z, c, q, own_tokens(q)).start()
+    locals_.append(pltpu.make_async_copy(tokens, whole(z, c), local_sem.at[0]))
+    scatter(1)
+    for kind in range(kinds):
+        locals_.append(pltpu.make_async_copy(own_columns(kind), stored(f, kind), local_sem.at[1]))
+    spots = ((gain_in, 0), (dgain_in, model), (sgain_in, model + dgain_in.shape[1]))
+    for source, first in spots:
         locals_.append(
-            pltpu.make_async_copy(own_tokens(q), held_at(z, c, q), local_sem.at[kinds + q])
-        )
-    for kind in range(kinds):
-        locals_.append(pltpu.make_async_copy(own_columns(kind), stored(f, kind), local_sem.at[kind]))
+            pltpu.make_async_copy(
+                source, gains.at[:, first : first + source.shape[1]], local_sem.at[2]
+            )
+        )
+    locals_.append(pltpu.make_async_copy(lam_in, lam_ref, local_sem.at[3]))
+    locals_.append(pltpu.make_async_copy(rate_in, rate_ref, local_sem.at[4]))
     for copy in locals_:
         copy.start()
 
@@ -393,26 +441,49 @@
         for way in range(2):
             kind = turn + way * half_kinds
             arrived(way, kind)
-            copy = spread(1 - way, kind, stored(whose[way], kind), whose[way], kinds + turn)
-            copy.start()
-            sends.append(copy)
-
-    def take(s, q):
-        for e in (1 + 2 * s, 2 + 2 * s):
-            b = slot(e)
-
-            @pl.when((b >= 0) & (b < line))
-            def _():
-                copy, _ = along(e, b, q)
-                copy.wait_recv()
-                if s + 1 < line - 1:
-                    onward, present = along(e + 2, b, q)
-
-                    @pl.when(present)
-                    def _():
-                        onward.start()
-
-                across(e, b, c, q).start()
+            spread(1 - way, kind, stored(whose[way], kind), whose[way], kinds + turn).start()
+
+    def complete(turn):
+        landed = weight.at[: 2 * depth, 2 * turn * width : 2 * (turn + 1) * width]
+        pltpu.make_async_remote_copy(
+            src_ref=landed,
+            dst_ref=landed,
+            send_sem=wsend,
+            recv_sem=wrecv.at[kinds + turn],
+            device_id=near[0],
+            device_id_type=MESH,
+        ).wait_recv()
+
+    def serve(e, q, when):
+        b = slot(e)
+
+        @pl.when((b >= 0) & (b < line) & when)
+        def _():
+            copy, _ = along(e, b, q)
+            copy.wait_recv()
+            if (e - 1) // 2 + 1 < line - 1:
+                onward, present = along(e + 2, b, q)
+
+                @pl.when(present)
+                def _():
+                    onward.start()
+
+            across(e, b, c, q).start()
+
+    def at_slot(k):
+        for s in range(line - 1):
+            for q in range(parts):
+                if q < early_parts:
+                    if k == s * early_parts + q:
+                        serve(1 + 2 * s, q, z > s)
+                else:
+                    for other in range(s + 1, line):
+                        if k == (2 * other - 4 - s) * early_parts + parts + q:
+                            serve(1 + 2 * s, q, z == other)
+        serve(2 + 2 * (k // parts), k % parts, z >= 0)
+        if k % parts == parts - 1 and k // parts < line - 2:
+            for q in range(early_parts, parts):
+                push(1, q, z == k // parts + 1)
 
     def fetch(index):
         source = index // 2
@@ -421,55 +492,95 @@
         return pltpu.make_async_copy(
             out_weight.at[first : first + width, :],
             held.at[source, kind * width : (kind + 1) * width, :],
-            held_sem.at[index],
+            held_sem,
         )
 
     fetches = [fetch(index) for index in range(2 * joined.shape[0])]
-    early = [(s, q) for s in range(line - 2) for q in range(parts)]
-    for turn in range(half_kinds):
-        relay(turn)
-        if turn == 0:
+
+    def block_of(e):
+        s = (e - 1) // 2
+        return jnp.where(e == 0, z, jnp.where((e - 1) % 2 == 0, z - 1 - s, z + 1 + s))
+
+    def rows_of(b):
+        return pl.ds(pl.multiple_of(b * block, block), block)
+
+    def normalize(e, b):
+        all_across(e, b).wait_recv()
+        x = seq[rows_of(b), :].astype(f32)
+        scaled = x * lax.rsqrt(jnp.mean(x * x, axis=1, keepdims=True) + epsilon)
+        normal[rows_of(b), :] = (scaled * gains[:, :model]).astype(bf16)
+
+    def project(b, pair):
+        columns = pl.ds(pl.multiple_of(pair * 2 * width, 2 * width), 2 * width)
+        proj[rows_of(b), columns] = jnp.dot(
+            normal[rows_of(b), :], weight[:, columns], preferred_element_type=f32
+        ).astype(bf16)
+
+    def soon(e, b):
+        return (e == 0) | (((e == 2) | ((e == 1) & (z == 1))) & (b < line))
+
+    def late(e):
+        return ((z == line - 1) & (e % 2 == 1) & (e < events - 2)) | ((z == 0) & (e == events - 1))
+
+    def first_pair(chosen):
+        def one(e, carry):
+            b = block_of(e)
+
+            @pl.when((b >= 0) & (b < line) & chosen(e, b))
+            def _():
+                normalize(e, b)
+                project(b, 0)
+
+            return carry
+
+        return one
+
+    def next_pair(pair):
+        def one(b, carry):
+            @pl.when(
+                ((z > 0) | (b < line - 1)) & ((z < line - 1) | (b == 0) | (b == line - 1))
+            )
+            def _():
+                project(b, pair)
+
+            return carry
+
+        lax.fori_loop(0, line, one, 0)
+
+    middle = parts + 1
+    early_slots = parts * (line - 2)
+    for k in range(early_slots):
+        at_slot(k)
+        if k == 0:
+            relay(0)
+            scatter(2)
             for copy in fetches:
                 copy.start()
-        elif early:
-            take(*early.pop(0))
-    for s, q in early:
-        take(s, q)
-    for copy in locals_:
-        copy.wait()
-    for kind in range(kinds):
-        for relation in range(3):
-            if relation == 2 or not (relation * half_kinds <= kind < (relation + 1) * half_kinds):
-                arrived(relation, kind)
-
-    def process(b):
-        rows = pl.ds(pl.multiple_of(b * block, block), block)
-        x = seq[rows, :].astype(f32)
-        scaled = x * lax.rsqrt(jnp.mean(x * x, axis=1, keepdims=True) + epsilon)
-        normed = (scaled * gain[...]).astype(bf16)
-        proj[rows, :] = jnp.dot(normed, weight[...], preferred_element_type=f32).astype(bf16)
-
-    def handle(e, carry):
-        up = (e - 1) % 2 == 0
-        s = (e - 1) // 2
-        b = jnp.where(e == 0, z, jnp.where(up, z - 1 - s, z + 1 + s))
-
-        @pl.when((b >= 0) & (b < line))
-        def _():
-            for q in range(parts):
-                across(e, b, 1 - c, q).wait_recv()
-            process(b)
-
-        return carry
+        if k == 2:
+            relay(1)
+        if k == middle:
+            relay(2)
+        if k == parts:
+            for copy in locals_[:1] + locals_[-2:]:
+                copy.wait()
+            mine_rows_in = weight.at[pl.ds(pl.multiple_of(f * depth, depth), depth), :]
+            pltpu.make_async_copy(mine_rows_in, mine_rows_in, local_sem.at[1]).wait()
+            pltpu.make_async_copy(gains, gains, local_sem.at[2]).wait()
+            complete(0)
+            lax.fori_loop(0, 3, first_pair(soon), 0)
+    complete(1)
+    lax.fori_loop(1, events, first_pair(lambda e, b: ~soon(e, b) & ~late(e)), 0)
+    next_pair(1)
+    complete(2)
+    next_pair(2)
 
     row = lax.broadcasted_iota(jnp.int32, (block, block), 0)
     col = lax.broadcasted_iota(jnp.int32, (block, block), 1)
     lane = lax.broadcasted_iota(jnp.int32, (block, 2 * DK), 1)
     position = lax.broadcasted_iota(jnp.int32, (block, 1), 0).astype(f32)
-    own_lanes = pl.ds(pl.multiple_of(z * DV, DV), DV)
 
     def part(kind, first, count):
-        return proj[first : first + count, kind * DV : kind * DV + DV]
+        return proj[first : first + count, column(kind) : column(kind) + DV]
 
     def mix(b):
         first = b * block
@@ -500,7 +611,7 @@
         differ = averaged[0] - lam * averaged[1]
         scaled = differ * lax.rsqrt(jnp.mean(differ * differ, axis=1, keepdims=True) + epsilon)
         mine[first : first + block, :DV] = (
-            scaled * (dgain_ref[:, own_lanes] * branch_scale)
+            scaled * (gains[:, pl.ds(pl.multiple_of(model + z * DV, DV), DV)] * branch_scale)
         ).astype(bf16)
         ret_query = part(3, first, block)
         ret_keys = part(4, first, block)
@@ -521,60 +632,98 @@
                 update = state[...] * jnp.exp(jnp.full((1, DR), -block, f32) * rate) + update
             state[...] = update
         scaled = mixed * lax.rsqrt(jnp.mean(mixed * mixed, axis=1, keepdims=True) + epsilon)
-        mine[first : first + block, DV:] = (scaled * sgain_ref[:, own_lanes]).astype(bf16)
+        mine[first : first + block, DV:] = (scaled * gains[:, pl.ds(pl.multiple_of(model + dgain_in.shape[1] + z * DV, DV), DV)]).astype(bf16)
 
     def mine_rows(b, side):
         return mine.at[pl.ds(pl.multiple_of(b * block + side * rows_out, rows_out), rows_out), :]
 
-    def deliver(b, turn):
-        side = c if turn == 0 else 1 - c
+    def deliver(b, h):
         return pltpu.make_async_remote_copy(
-            src_ref=mine_rows(b, side),
+            src_ref=mine_rows(b, h),
             dst_ref=joined.at[me],
-            send_sem=osend.at[b, turn],
+            send_sem=osend,
             recv_sem=orecv.at[me],
-            device_id={"sp": b, "tp": side},
+            device_id={"sp": b, "tp": h},
             device_id_type=MESH,
         )
 
+    def own_place(b, h):
+        return (z == b) & (c == h)
+
+    def send(b, when):
+        for h in range(2):
+
+            @pl.when(when & ~own_place(b, h))
+            def _():
+                deliver(b, h).start()
+
     def give(b):
-        deliver(b, 1).start()
-
-        @pl.when(z != b)
-        def _():
-            deliver(b, 0).start()
+        if b == 0:
+            send(b, z == 0)
+        elif b == line - 1:
+            send(b, (z == 0) | (z == line - 1))
+        else:
+            send(b, z >= 0)
 
         @pl.when(z == b)
         def _():
             joined[me] = mine_rows(b, c)[...]
 
-    last = 2 * line - 3
-    lax.fori_loop(0, last, handle, 0)
+    def last_token(end):
+        if end == 0:
+            return all_along(events - 1), z == 1
+        return all_along(1), z == line - 2
 
     def phase(t, carry):
-        @pl.when(t == 1)
+        @pl.when(t == line - 2)
         def _():
-            for q in range(parts):
-                take(line - 2, q)
-            lax.fori_loop(last, last + 2, handle, 0)
+            for end in (0, line - 1):
+                copy, here = last_token(end)
+
+                @pl.when(here)
+                def _():
+                    copy.wait_send()
+
+            send(0, z > 0)
+            send(line - 1, (z > 0) & (z < line - 1))
+
+        for turn in range(1, line - 1):
+
+            @pl.when(t == turn)
+            def _():
+                for q in range(early_parts):
+                    at_slot(early_slots + (turn - 1) * early_parts + q)
+
+        @pl.when((t > 0) & ((z == line - 1) | ((z == 0) & (t == line - 2))))
+        def _():
+            b = jnp.where(z == 0, line - 1, t)
+            e = jnp.where(z == 0, events - 1, 2 * (line - 2 - t) + 1)
+            normalize(e, b)
+            for pair in range(half_kinds):
+                project(b, pair)
 
         for b in range(line):
-            late = z == line - 1
+            turn = jnp.where(z == line - 1, min(b, line - 2), 0)
             if b == line - 1:
-                late = late | (z == 0)
-
-            @pl.when(late == (t == 1))
+                turn = jnp.where(z == 0, line - 2, turn)
+
+            @pl.when(turn == t)
             def _():
                 mix(b)
                 give(b)
 
         return carry
 
-    lax.fori_loop(0, 2, phase, 0)
-
-    for copy in fetches:
-        copy.wait()
-    order = [s for s in range(1, line - 1)] + [0, line - 1]
+    lax.fori_loop(0, line - 1, phase, 0)
+
+    pltpu.make_async_copy(held, held, held_sem).wait()
+    inner = [s for s in range(1, line - 1)]
+    outer = (z == 0) | (z == line - 1)
+    order = []
+    for index in range(line):
+        for_outer = ([0, line - 1] + inner)[index]
+        for_inner = (inner + [0, line - 1])[index]
+        order.append(jnp.where(outer, for_outer, for_inner))
     for index, source in enumerate(order):
         for turn in range(2):
             side = c if turn == 0 else 1 - c
@@ -585,7 +734,7 @@
                 pltpu.make_async_remote_copy(
                     src_ref=joined.at[where],
                     dst_ref=joined.at[where],
-                    send_sem=osend.at[0, 0],
+                    send_sem=osend,
                     recv_sem=orecv.at[where],
                     device_id={"tp": 1 - c},
                     device_id_type=MESH,
@@ -599,37 +748,47 @@
             else:
                 result[...] = (total[...] + product).astype(bf16)
 
-    for copy in sends:
-        copy.wait_send()
-    for q in range(parts):
-        across(0, z, c, q, own_tokens(q)).wait_send()
-        for e in (1, 2):
-            copy, present = along(e, z, q, own_tokens(q))
-
-            @pl.when(present)
-            def _():
-                copy.wait_send()
-
-        for s in range(line - 1):
-            for e in (1 + 2 * s, 2 + 2 * s):
-                b = slot(e)
-
-                @pl.when((b >= 0) & (b < line))
-                def _():
-                    across(e, b, c, q).wait_send()
-                    if s + 1 < line - 1:
-                        onward, present = along(e + 2, b, q)
-
-                        @pl.when(present)
-                        def _():
-                            onward.wait_send()
-
-    for b in range(line):
-        deliver(b, 1).wait_send()
-
-        @pl.when(z != b)
+    sent = weight.at[: 3 * depth, :]
+    pltpu.make_async_remote_copy(
+        src_ref=sent,
+        dst_ref=sent,
+        send_sem=wsend,
+        recv_sem=wrecv.at[0],
+        device_id=near[0],
+        device_id_type=MESH,
+    ).wait_send()
+    for e in range(events):
+        b = block_of(e)
+
+        @pl.when((b >= 0) & (b < line))
         def _():
-            deliver(b, 0).wait_send()
+            all_across(e, b).wait_send()
+
+        if e == 0:
+            continue
+        up = e % 2 == 1
+        target = z + 1 if up else z - 1
+        s = (e - 1) // 2
+        source = z - s if up else z + s
+        present = (target >= 0) & (target < line) & (source >= 0) & (source < line)
+        if e == 1:
+            present = present & (z != line - 2)
+        if e == events - 1:
+            present = present & (z != 1)
+
+        @pl.when(present)
+        def _():
+            all_along(e).wait_send()
+
+    gone = mine.at[: (2 * line - 1) * rows_out, :]
+    pltpu.make_async_remote_copy(
+        src_ref=gone,
+        dst_ref=gone,
+        send_sem=osend,
+        recv_sem=orecv.at[0],
+        device_id={"tp": 1 - c},
+        device_id_type=MESH,
+    ).wait_send()
 
 
 def whole_layer(tokens, norm_gain, weights, map_lambda, diff_gain, decay_rate, state_gain, out_weight, line, pair):
@@ -641,16 +800,19 @@
     count = line * pair
     anywhere = pl.BlockSpec(memory_space=pl.ANY)
     vmem = pl.BlockSpec(memory_space=pltpu.VMEM)
-    smem = pl.BlockSpec(memory_space=pltpu.SMEM)
     events = 2 * line - 1
     dma = pltpu.SemaphoreType.DMA
     bf16 = jnp.bfloat16
     return pl.pallas_call(
         functools.partial(layer_kernel, line, parts),
         out_shape=jax.ShapeDtypeStruct((rows, out_weight.shape[1]), bf16),
-        in_specs=[anywhere, vmem] + [anywhere] * kinds + [smem, vmem, smem, vmem, anywhere],
+        in_specs=[anywhere] * (kinds + 7),
         out_specs=vmem,
         scratch_shapes=[
+            pltpu.VMEM((1, model + diff_gain.shape[0] + state_gain.shape[0]), jnp.float32),
+            pltpu.SMEM(map_lambda.shape, jnp.float32),
+            pltpu.SMEM(decay_rate.shape, jnp.float32),
+            pltpu.VMEM((line * block, model), bf16),
             pltpu.VMEM((line * block, model), bf16),
             pltpu.VMEM((model, kinds * DV), bf16),
             pltpu.VMEM((line * block, kinds * DV), bf16),
@@ -659,15 +821,15 @@
             pltpu.VMEM((count, 2 * DV, out_weight.shape[1]), bf16),
             pltpu.VMEM((DR, DR), jnp.float32),
             pltpu.VMEM((rows, out_weight.shape[1]), jnp.float32),
-            dma((kinds + parts,)),
-            dma((2 * count,)),
-            dma((2, kinds + kinds // 2)),
-            dma((3, kinds)),
+            dma((5,)),
+            dma,
+            dma,
+            dma((kinds + kinds // 2,)),
+            dma((events,)),
             dma((events, parts)),
-            dma((events, parts)),
-            dma((events, parts)),
-            dma((events, parts)),
-            dma((line, pair)),
+            dma((events,)),
+            dma((events,)),
+            dma,
             dma((count,)),
         ],
         compiler_params=pltpu.CompilerParams(
@@ -690,7 +852,7 @@
     line = lax.axis_size("sp")
     pair = lax.axis_size("tp")
     local = map_lambda.shape[0]
-    if local != line or decay_rate.shape[0] != local or lax.axis_size("fs") != 4 or pair != 2:
+    if local != line or line < 3 or decay_rate.shape[0] != local or lax.axis_size("fs") != 4 or pair != 2:
         return spread_body(tokens, norm_gain, *rest)
     return whole_layer(
         tokens[0],

time: 55.5 us -> 53.4 us (0.962)
  the two profiles are of different devices: /device:TPU:17 before, /device:TPU:1 now
where the time goes in v2:
time: 53.4 us; the launch traced here: 53.2 us
  Pallas kernels  51.3 us (96%)
  local copies, waits for them, and re-layouts  1.88 us (4%)
    pallas_call x1, Pallas kernels, whole_layer(): pl.pallas_call(functools.partial(layer_kernel, line, parts), out_shape=ja...  51.3 us
    unnamed x1, local copies, waits for them, and re-layouts  1.88 us

profile of v2, /device:TPU:1, one launch (start us, length us, event | category | flops | bytes accessed | tf_op | source)
XLA Modules:
  0.0 53.2 jit_solution(6093603255557074783)
XLA Ops:
  0.0 51.3 %shard_map.127 = bf16[128,2048]{1,0:T(8,128)(2,1)} custom-call(bf16[256,1024]{1,0:T(8,128)(2,1)} %bitcast.6, f32[1,2048]{1,0:T(1,128)} %bitcast.7, bf16[512,512]{1,0:T(8,128)(2,1)} %w0.1, bf16[512,512]{1,0:T(8,128)(2,1)} %w1.1, bf16[512,512]{1,0:T(8,128)(2,1)} %w2.1, bf16[512,512]{1,0:T(8,128)(2,1)} %w3.1, bf16[512,512]{1,0:T(8,128)(2,1)} %w4.1, ...), custom_call_target="tpu_custom_call" | custom-call | tf_op jit(solution)/shard_map/pallas_call | solution.py:806
  51.4 1.9 %copy.15 = bf16[1,128,2048]{2,1,0:T(8,128)(2,1)} copy(bf16[1,128,2048]{2,1,0:T(8,128)(2,1)} %bitcast.5) | data formatting | bytes 1048576

commit v3 on v2

--- a/solution.py
+++ b/solution.py
@@ -297,16 +297,6 @@
     me = c * line + z
     near = ({"fs": f ^ 1}, {"fs": f ^ 2})
     whose = (f ^ 1, f ^ 2, f ^ 3)
-    greet(
-        [
-            (near[0], None),
-            (near[1], None),
-            ({"tp": 1 - c}, None),
-            ({"sp": jnp.minimum(z + 1, line - 1)}, z + 1 < line),
-            ({"sp": jnp.maximum(z - 1, 0)}, z > 0),
-        ]
-    )
-
     def held_at(b, side, q):
         return seq.at[
             pl.ds(pl.multiple_of(b * block + q * piece, piece), piece),
@@ -319,9 +309,6 @@
             pl.ds(pl.multiple_of(side * half, half), half),
         ]
 
-    def own_tokens(q):
-        return tokens.at[q * piece : (q + 1) * piece, :]
-
     def column(kind):
         return (2 * (kind % half_kinds) + kind // half_kinds) * width
 
@@ -335,10 +322,10 @@
         s = (e - 1) // 2
         return z - 1 - s if up else z + 1 + s
 
-    def along(e, b, q, source=None):
+    def along(e, b, q):
         target = z + 1 if (e - 1) % 2 == 0 else z - 1
         return pltpu.make_async_remote_copy(
-            src_ref=held_at(b, c, q) if source is None else source,
+            src_ref=held_at(b, c, q),
             dst_ref=held_at(b, c, q),
             send_sem=lsend.at[e],
             recv_sem=lrecv.at[e, q],
@@ -346,9 +333,9 @@
             device_id_type=MESH,
         ), (target >= 0) & (target < line)
 
-    def across(e, b, side, q, source=None):
+    def across(e, b, side, q):
         return pltpu.make_async_remote_copy(
-            src_ref=held_at(b, side, q) if source is None else source,
+            src_ref=held_at(b, side, q),
             dst_ref=held_at(b, side, q),
             send_sem=psend.at[e],
             recv_sem=precv.at[e],
@@ -358,7 +345,7 @@
 
     def all_along(e):
         return pltpu.make_async_remote_copy(
-            src_ref=tokens,
+            src_ref=whole(z, c),
             dst_ref=whole(z, c),
             send_sem=lsend.at[e],
             recv_sem=lrecv.at[e, 0],
@@ -403,38 +390,54 @@
         ).wait_recv()
 
     def push(e, q, when=True):
-        copy, present = along(e, z, q, own_tokens(q))
+        copy, present = along(e, z, q)
 
         @pl.when(present & when)
         def _():
             copy.start()
 
     def scatter(pair):
-        for kind in (pair, pair + half_kinds):
+        for turn in range(2):
             for way in range(2):
-                spread(way, kind, own_columns(kind), f, kind).start()
-
+                kind = pair + half_kinds * (turn ^ way)
+                spread(way, kind, stored(f, kind), f, kind).start()
+
+    first_copies = [pltpu.make_async_copy(tokens, whole(z, c), local_sem.at[0])]
+    for kind in range(kinds):
+        first_copies.append(
+            pltpu.make_async_copy(own_columns(kind), stored(f, kind), local_sem.at[1])
+        )
+    for copy in first_copies:
+        copy.start()
+    greet(
+        [
+            (near[0], None),
+            (near[1], None),
+            ({"tp": 1 - c}, None),
+            ({"sp": jnp.minimum(z + 1, line - 1)}, z + 1 < line),
+            ({"sp": jnp.maximum(z - 1, 0)}, z > 0),
+        ]
+    )
+    first_copies[0].wait()
     for q in range(parts):
         push(1, q, z >= 0 if q < early_parts else z == 0)
         push(2, q)
+    own_rows = weight.at[pl.ds(pl.multiple_of(f * depth, depth), depth), :]
+    pltpu.make_async_copy(own_rows, own_rows, local_sem.at[1]).wait()
     scatter(0)
-    locals_ = []
     for q in range(parts):
-        across(0, z, c, q, own_tokens(q)).start()
-    locals_.append(pltpu.make_async_copy(tokens, whole(z, c), local_sem.at[0]))
+        across(0, z, c, q).start()
     scatter(1)
-    for kind in range(kinds):
-        locals_.append(pltpu.make_async_copy(own_columns(kind), stored(f, kind), local_sem.at[1]))
     spots = ((gain_in, 0), (dgain_in, model), (sgain_in, model + dgain_in.shape[1]))
     for source, first in spots:
-        locals_.append(
-            pltpu.make_async_copy(
-                source, gains.at[:, first : first + source.shape[1]], local_sem.at[2]
-            )
-        )
-    locals_.append(pltpu.make_async_copy(lam_in, lam_ref, local_sem.at[3]))
-    locals_.append(pltpu.make_async_copy(rate_in, rate_ref, local_sem.at[4]))
-    for copy in locals_:
+        pltpu.make_async_copy(
+            source, gains.at[:, first : first + source.shape[1]], local_sem.at[2]
+        ).start()
+    rates = (
+        pltpu.make_async_copy(lam_in, lam_ref, local_sem.at[3]),
+        pltpu.make_async_copy(rate_in, rate_ref, local_sem.at[4]),
+    )
+    for copy in rates:
         copy.start()
 
     def relay(turn):
@@ -510,8 +513,8 @@
         scaled = x * lax.rsqrt(jnp.mean(x * x, axis=1, keepdims=True) + epsilon)
         normal[rows_of(b), :] = (scaled * gains[:, :model]).astype(bf16)
 
-    def project(b, pair):
-        columns = pl.ds(pl.multiple_of(pair * 2 * width, 2 * width), 2 * width)
+    def project(b, first, count):
+        columns = slice(2 * first * width, 2 * (first + count) * width)
         proj[rows_of(b), columns] = jnp.dot(
             normal[rows_of(b), :], weight[:, columns], preferred_element_type=f32
         ).astype(bf16)
@@ -522,57 +525,50 @@
     def late(e):
         return ((z == line - 1) & (e % 2 == 1) & (e < events - 2)) | ((z == 0) & (e == events - 1))
 
-    def first_pair(chosen):
+    def normalize_some(first, last, chosen):
         def one(e, carry):
             b = block_of(e)
 
             @pl.when((b >= 0) & (b < line) & chosen(e, b))
             def _():
                 normalize(e, b)
-                project(b, 0)
 
             return carry
 
-        return one
-
-    def next_pair(pair):
+        lax.fori_loop(first, last, one, 0)
+
+    def project_ready(first, count):
         def one(b, carry):
             @pl.when(
                 ((z > 0) | (b < line - 1)) & ((z < line - 1) | (b == 0) | (b == line - 1))
             )
             def _():
-                project(b, pair)
+                project(b, first, count)
 
             return carry
 
         lax.fori_loop(0, line, one, 0)
 
-    middle = parts + 1
     early_slots = parts * (line - 2)
+    relay(0)
+    scatter(2)
+    for copy in fetches:
+        copy.start()
     for k in range(early_slots):
         at_slot(k)
-        if k == 0:
-            relay(0)
-            scatter(2)
-            for copy in fetches:
-                copy.start()
-        if k == 2:
-            relay(1)
-        if k == middle:
-            relay(2)
+        if k < 2:
+            relay(k + 1)
         if k == parts:
-            for copy in locals_[:1] + locals_[-2:]:
+            for copy in rates:
                 copy.wait()
-            mine_rows_in = weight.at[pl.ds(pl.multiple_of(f * depth, depth), depth), :]
-            pltpu.make_async_copy(mine_rows_in, mine_rows_in, local_sem.at[1]).wait()
             pltpu.make_async_copy(gains, gains, local_sem.at[2]).wait()
-            complete(0)
-            lax.fori_loop(0, 3, first_pair(soon), 0)
-    complete(1)
-    lax.fori_loop(1, events, first_pair(lambda e, b: ~soon(e, b) & ~late(e)), 0)
-    next_pair(1)
-    complete(2)
-    next_pair(2)
+            normalize_some(0, 3, soon)
+    normalize_some(1, events, lambda e, b: ~soon(e, b) & ~late(e))
+    for turn in range(half_kinds - 1):
+        complete(turn)
+    project_ready(0, half_kinds - 1)
+    complete(half_kinds - 1)
+    project_ready(half_kinds - 1, 1)
 
     row = lax.broadcasted_iota(jnp.int32, (block, block), 0)
     col = lax.broadcasted_iota(jnp.int32, (block, block), 1)
@@ -659,9 +655,9 @@
 
     def give(b):
         if b == 0:
-            send(b, z == 0)
+            send(b, z <= 1)
         elif b == line - 1:
-            send(b, (z == 0) | (z == line - 1))
+            send(b, (z == 0) | (z >= line - 2))
         else:
             send(b, z >= 0)
 
@@ -684,8 +680,8 @@
                 def _():
                     copy.wait_send()
 
-            send(0, z > 0)
-            send(line - 1, (z > 0) & (z < line - 1))
+            send(0, z > 1)
+            send(line - 1, (z > 0) & (z < line - 2))
 
         for turn in range(1, line - 1):
 
@@ -699,8 +695,7 @@
             b = jnp.where(z == 0, line - 1, t)
             e = jnp.where(z == 0, events - 1, 2 * (line - 2 - t) + 1)
             normalize(e, b)
-            for pair in range(half_kinds):
-                project(b, pair)
+            project(b, 0, half_kinds)
 
         for b in range(line):
             turn = jnp.where(z == line - 1, min(b, line - 2), 0)
@@ -803,6 +798,16 @@
     events = 2 * line - 1
     dma = pltpu.SemaphoreType.DMA
     bf16 = jnp.bfloat16
+    operands = (
+        tokens,
+        norm_gain[None],
+        *weights,
+        map_lambda,
+        diff_gain[None],
+        decay_rate,
+        state_gain[None],
+        out_weight,
+    )
     return pl.pallas_call(
         functools.partial(layer_kernel, line, parts),
         out_shape=jax.ShapeDtypeStruct((rows, out_weight.shape[1]), bf16),
@@ -833,17 +838,10 @@
             dma((count,)),
         ],
         compiler_params=pltpu.CompilerParams(
-            collective_id=0, has_side_effects=True, vmem_limit_bytes=65000 * 1024
+            collective_id=0, has_side_effects=True, vmem_limit_bytes=40000 * 1024
         ),
     )(
-        tokens,
-        norm_gain[None],
-        *weights,
-        map_lambda,
-        diff_gain[None],
-        decay_rate,
-        state_gain[None],
-        out_weight,
+        *(pltpu.with_memory_space_constraint(a, pltpu.HBM) for a in operands)
     )
 
 

time: 53.4 us -> 51.8 us (0.970)
  local copies, waits for them, and re-layouts: 1.88 us -> 0.8 us
    unnamed x1, local copies, waits for them, and re-layouts: 1.88 us -> 0.8 us
where the time goes in v3:
time: 51.8 us; the launch traced here: 51.7 us
  Pallas kernels  50.9 us (98%)
  local copies, waits for them, and re-layouts  0.8 us (2%)
    pallas_call x1, Pallas kernels, whole_layer(): pl.pallas_call(functools.partial(layer_kernel, line, parts), out_shape=ja...  50.9 us

profile of v3, /device:TPU:1, one launch (start us, length us, event | category | flops | bytes accessed | tf_op | source)
XLA Modules:
  0.0 51.7 jit_solution(4599033084277989017)
XLA Ops:
  0.0 50.9 %shard_map.127 = bf16[128,2048]{1,0:T(8,128)(2,1)S(1)} custom-call(bf16[256,1024]{1,0:T(8,128)(2,1)} %bitcast.6, f32[1,2048]{1,0:T(1,128)} %bitcast.7, bf16[512,512]{1,0:T(8,128)(2,1)} %w0.1, bf16[512,512]{1,0:T(8,128)(2,1)} %w1.1, bf16[512,512]{1,0:T(8,128)(2,1)} %w2.1, bf16[512,512]{1,0:T(8,128)(2,1)} %w3.1, bf16[512,512]{1,0:T(8,128)(2,1)} %w4.1, ...), custom_call_target="tpu_custom_call" | custom-call | tf_op jit(solution)/shard_map/pallas_call | solution.py:811
  50.9 0.8 %copy.15 = bf16[1,128,2048]{2,1,0:T(8,128)(2,1)} copy(bf16[1,128,2048]{2,1,0:T(8,128)(2,1)S(1)} %bitcast.5) | data formatting | bytes 1048576

commit v4 on v3

--- a/solution.py
+++ b/solution.py
@@ -338,7 +338,7 @@
             src_ref=held_at(b, side, q),
             dst_ref=held_at(b, side, q),
             send_sem=psend.at[e],
-            recv_sem=precv.at[e],
+            recv_sem=precv.at[e, q],
             device_id={"tp": 1 - c},
             device_id_type=MESH,
         )
@@ -358,7 +358,7 @@
             src_ref=whole(b, 1 - c),
             dst_ref=whole(b, 1 - c),
             send_sem=psend.at[e],
-            recv_sem=precv.at[e],
+            recv_sem=precv.at[e, 0],
             device_id={"tp": 1 - c},
             device_id_type=MESH,
         )
@@ -508,7 +508,8 @@
         return pl.ds(pl.multiple_of(b * block, block), block)
 
     def normalize(e, b):
-        all_across(e, b).wait_recv()
+        for q in range(parts):
+            across(e, b, 1 - c, q).wait_recv()
         x = seq[rows_of(b), :].astype(f32)
         scaled = x * lax.rsqrt(jnp.mean(x * x, axis=1, keepdims=True) + epsilon)
         normal[rows_of(b), :] = (scaled * gains[:, :model]).astype(bf16)
@@ -646,8 +647,8 @@
     def own_place(b, h):
         return (z == b) & (c == h)
 
-    def send(b, when):
-        for h in range(2):
+    def send(b, when, halves=(0, 1)):
+        for h in halves:
 
             @pl.when(when & ~own_place(b, h))
             def _():
@@ -680,8 +681,13 @@
                 def _():
                     copy.wait_send()
 
-            send(0, z > 1)
+            send(0, (z > 1) & (z < line - 1))
+            send(0, z == line - 1, (1,))
             send(line - 1, (z > 0) & (z < line - 2))
+
+        @pl.when(t == line - 3)
+        def _():
+            send(0, z == line - 1, (0,))
 
         for turn in range(1, line - 1):
 
@@ -690,12 +696,25 @@
                 for q in range(early_parts):
                     at_slot(early_slots + (turn - 1) * early_parts + q)
 
-        @pl.when((t > 0) & ((z == line - 1) | ((z == 0) & (t == line - 2))))
+        @pl.when((t > 0) & ((z == line - 1) | ((z == 0) & (t <= parts))))
         def _():
             b = jnp.where(z == 0, line - 1, t)
             e = jnp.where(z == 0, events - 1, 2 * (line - 2 - t) + 1)
-            normalize(e, b)
-            project(b, 0, half_kinds)
+
+            def one(q, carry):
+                across(e, b, 1 - c, q).wait_recv()
+                rows = pl.ds(pl.multiple_of(b * block + q * piece, piece), piece)
+                x = seq[rows, :].astype(f32)
+                scaled = x * lax.rsqrt(jnp.mean(x * x, axis=1, keepdims=True) + epsilon)
+                normal[rows, :] = (scaled * gains[:, :model]).astype(bf16)
+                proj[rows, :] = jnp.dot(
+                    normal[rows, :], weight[...], preferred_element_type=f32
+                ).astype(bf16)
+                return carry
+
+            lax.fori_loop(
+                jnp.where(z == 0, t - 1, 0), jnp.where(z == 0, t, parts), one, 0
+            )
 
         for b in range(line):
             turn = jnp.where(z == line - 1, min(b, line - 2), 0)
@@ -833,7 +852,7 @@
             dma((events,)),
             dma((events, parts)),
             dma((events,)),
-            dma((events,)),
+            dma((events, parts)),
             dma,
             dma((count,)),
         ],
@@ -850,7 +869,7 @@
     line = lax.axis_size("sp")
     pair = lax.axis_size("tp")
     local = map_lambda.shape[0]
-    if local != line or line < 3 or decay_rate.shape[0] != local or lax.axis_size("fs") != 4 or pair != 2:
+    if local != line or line < 4 or decay_rate.shape[0] != local or lax.axis_size("fs") != 4 or pair != 2:
         return spread_body(tokens, norm_gain, *rest)
     return whole_layer(
         tokens[0],

time: 51.8 us -> 50.9 us (0.983)
  Pallas kernels: 50.9 us -> 49.9 us
    pallas_call x1, Pallas kernels: 50.9 us -> 49.9 us  [whole_layer(): pl.pallas_call(functools.partial(layer_kernel, line, parts), out_shape=ja...]
where the time goes in v4:
time: 50.9 us; the launch traced here: 50.7 us
  Pallas kernels  49.9 us (98%)
  local copies, waits for them, and re-layouts  0.8 us (2%)
    pallas_call x1, Pallas kernels, whole_layer(): pl.pallas_call(functools.partial(layer_kernel, line, parts), out_shape=ja...  49.9 us

profile of v4, /device:TPU:1, one launch (start us, length us, event | category | flops | bytes accessed | tf_op | source)
XLA Modules:
  0.0 50.7 jit_solution(1172174537232583063)
XLA Ops:
  0.0 49.9 %shard_map.127 = bf16[128,2048]{1,0:T(8,128)(2,1)S(1)} custom-call(bf16[256,1024]{1,0:T(8,128)(2,1)} %bitcast.6, f32[1,2048]{1,0:T(1,128)} %bitcast.7, bf16[512,512]{1,0:T(8,128)(2,1)} %w0.1, bf16[512,512]{1,0:T(8,128)(2,1)} %w1.1, bf16[512,512]{1,0:T(8,128)(2,1)} %w2.1, bf16[512,512]{1,0:T(8,128)(2,1)} %w3.1, bf16[512,512]{1,0:T(8,128)(2,1)} %w4.1, ...), custom_call_target="tpu_custom_call" | custom-call | tf_op jit(solution)/shard_map/pallas_call | solution.py:830
  49.9 0.8 %copy.15 = bf16[1,128,2048]{2,1,0:T(8,128)(2,1)} copy(bf16[1,128,2048]{2,1,0:T(8,128)(2,1)S(1)} %bitcast.5) | data formatting | bytes 1048576

commit v5 on v4

--- a/solution.py
+++ b/solution.py
@@ -337,7 +337,7 @@
         return pltpu.make_async_remote_copy(
             src_ref=held_at(b, side, q),
             dst_ref=held_at(b, side, q),
-            send_sem=psend.at[e],
+            send_sem=psend,
             recv_sem=precv.at[e, q],
             device_id={"tp": 1 - c},
             device_id_type=MESH,
@@ -353,12 +353,13 @@
             device_id_type=MESH,
         )
 
-    def all_across(e, b):
+    def all_across():
+        columns = seq.at[:, pl.ds(pl.multiple_of(c * half, half), half)]
         return pltpu.make_async_remote_copy(
-            src_ref=whole(b, 1 - c),
-            dst_ref=whole(b, 1 - c),
-            send_sem=psend.at[e],
-            recv_sem=precv.at[e, 0],
+            src_ref=columns,
+            dst_ref=columns,
+            send_sem=psend,
+            recv_sem=precv.at[0, 0],
             device_id={"tp": 1 - c},
             device_id_type=MESH,
         )
@@ -666,21 +667,9 @@
         def _():
             joined[me] = mine_rows(b, c)[...]
 
-    def last_token(end):
-        if end == 0:
-            return all_along(events - 1), z == 1
-        return all_along(1), z == line - 2
-
     def phase(t, carry):
         @pl.when(t == line - 2)
         def _():
-            for end in (0, line - 1):
-                copy, here = last_token(end)
-
-                @pl.when(here)
-                def _():
-                    copy.wait_send()
-
             send(0, (z > 1) & (z < line - 1))
             send(0, z == line - 1, (1,))
             send(line - 1, (z > 0) & (z < line - 2))
@@ -729,6 +718,27 @@
         return carry
 
     lax.fori_loop(0, line - 1, phase, 0)
+
+    sent = weight.at[: 3 * depth, :]
+    pltpu.make_async_remote_copy(
+        src_ref=sent,
+        dst_ref=sent,
+        send_sem=wsend,
+        recv_sem=wrecv.at[0],
+        device_id=near[0],
+        device_id_type=MESH,
+    ).wait_send()
+    all_across().wait_send()
+    for e in range(1, events):
+        up = e % 2 == 1
+        target = z + 1 if up else z - 1
+        s = (e - 1) // 2
+        source = z - s if up else z + s
+        present = (target >= 0) & (target < line) & (source >= 0) & (source < line)
+
+        @pl.when(present)
+        def _():
+            all_along(e).wait_send()
 
     pltpu.make_async_copy(held, held, held_sem).wait()
     inner = [s for s in range(1, line - 1)]
@@ -761,38 +771,6 @@
                 total[...] += product
             else:
                 result[...] = (total[...] + product).astype(bf16)
-
-    sent = weight.at[: 3 * depth, :]
-    pltpu.make_async_remote_copy(
-        src_ref=sent,
-        dst_ref=sent,
-        send_sem=wsend,
-        recv_sem=wrecv.at[0],
-        device_id=near[0],
-        device_id_type=MESH,
-    ).wait_send()
-    for e in range(events):
-        b = block_of(e)
-
-        @pl.when((b >= 0) & (b < line))
-        def _():
-            all_across(e, b).wait_send()
-
-        if e == 0:
-            continue
-        up = e % 2 == 1
-        target = z + 1 if up else z - 1
-        s = (e - 1) // 2
-        source = z - s if up else z + s
-        present = (target >= 0) & (target < line) & (source >= 0) & (source < line)
-        if e == 1:
-            present = present & (z != line - 2)
-        if e == events - 1:
-            present = present & (z != 1)
-
-        @pl.when(present)
-        def _():
-            all_along(e).wait_send()
 
     gone = mine.at[: (2 * line - 1) * rows_out, :]
     pltpu.make_async_remote_copy(
@@ -851,7 +829,7 @@
             dma((kinds + kinds // 2,)),
             dma((events,)),
             dma((events, parts)),
-            dma((events,)),
+            dma,
             dma((events, parts)),
             dma,
             dma((count,)),

time: 50.9 us -> 50.8 us (level)
  no operation moved by 1% of the time
where the time goes in v5:
time: 50.8 us; the launch traced here: 50.6 us
  Pallas kernels  49.8 us (98%)
  local copies, waits for them, and re-layouts  0.8 us (2%)
    pallas_call x1, Pallas kernels, whole_layer(): pl.pallas_call(functools.partial(layer_kernel, line, parts), out_shape=ja...  49.8 us

profile of v5, /device:TPU:1, one launch (start us, length us, event | category | flops | bytes accessed | tf_op | source)
XLA Modules:
  0.0 50.6 jit_solution(17420620186744685553)
XLA Ops:
  0.0 49.8 %shard_map.127 = bf16[128,2048]{1,0:T(8,128)(2,1)S(1)} custom-call(bf16[256,1024]{1,0:T(8,128)(2,1)} %bitcast.6, f32[1,2048]{1,0:T(1,128)} %bitcast.7, bf16[512,512]{1,0:T(8,128)(2,1)} %w0.1, bf16[512,512]{1,0:T(8,128)(2,1)} %w1.1, bf16[512,512]{1,0:T(8,128)(2,1)} %w2.1, bf16[512,512]{1,0:T(8,128)(2,1)} %w3.1, bf16[512,512]{1,0:T(8,128)(2,1)} %w4.1, ...), custom_call_target="tpu_custom_call" | custom-call | tf_op jit(solution)/shard_map/pallas_call | solution.py:808
  49.8 0.8 %copy.15 = bf16[1,128,2048]{2,1,0:T(8,128)(2,1)} copy(bf16[1,128,2048]{2,1,0:T(8,128)(2,1)S(1)} %bitcast.5) | data formatting | bytes 1048576
